TPU v7x, 32 devices: a whole 2x2x4 slice. The times are simulated.
32 devices in a mesh: sp: 8 (over z, x), tp: 4 (over y, core).
Axes of the slice: x: 2, y: 2, z: 4, core: 2. Of those that a mesh axis runs over, the one named last changes fastest.
Arguments:
- tokens: bfloat16 [3072, 2048], P('sp', 'tp'), may hold values from -6 to 6
- norm_gain: float32 [2048], replicated, may hold values from 0.1 to 1.9
- w_pool_in: bfloat16 [2048, 2048], P('sp', 'tp'), may hold values from -0.125 to 0.125
- w_lru_in: bfloat16 [2048, 2048], P('sp', 'tp'), may hold values from -0.125 to 0.125
- pool_mix: bfloat16 [4, 512, 512], P('tp'), may hold values from -0.25 to 0.25
- conv_taps: bfloat16 [4, 2048], P(None, 'tp'), may hold values from -3 to 3
- rec_gate: bfloat16 [2, 16, 128, 128], P(None, 'tp'), may hold values from -0.5 to 0.5
- in_gate: bfloat16 [2, 16, 128, 128], P(None, 'tp'), may hold values from -0.5 to 0.5
- decay_rate: float32 [2, 2048], P(None, 'tp'), may hold values from 0 to 1, as said below
- log_decay: float32 [2, 3072], P(None, 'sp'), may hold values from -2 to 0, as said below
- start_state: float32 [2, 2048], P(None, 'tp'), may hold values from -8 to 8
- w_out_pool: bfloat16 [2048, 2048], P('tp', 'sp'), may hold values from -0.09375 to 0.09375
- w_out_lru: bfloat16 [2048, 2048], P('tp', 'sp'), may hold values from -0.09375 to 0.09375
Outputs:
- mixed: bfloat16 [3072, 2048], P(('sp', 'tp'))
Inputs may be any that keep to these rules, and one draw needn't show every extreme that they name: `decay_rate`: positive. `log_decay`: at most zero.
All inputs are finite; a program needn't handle non-finite values.
Results may differ from a plain program's by a relative error of at most 0.0068.
Values may be sent and summed in bfloat16 or wider, within the bound.
A program may use at most 64 MiB of HBM per device.

v0:
```python
import functools

import jax
import jax.numpy as jnp
from jax import lax
from jax.experimental import pallas as pl
from jax.experimental.pallas import tpu as pltpu
from jax.sharding import PartitionSpec as P

POOL_GROUPS = 4
GRID_W = 32
REACH = 2 ** (POOL_GROUPS - 1)
EPSILON = 1e-06
EDGE = 16
CHUNKS = 8


def one_minus_exp(y):
    series = jnp.full_like(y, 1.0 / 40320.0)
    for factorial in (5040.0, 720.0, 120.0, 24.0, 6.0, 2.0, 1.0):
        series = series * y + 1.0 / factorial
    return jnp.where(y > -0.35, -y * series, 1.0 - jnp.exp(y))


def pool_stage(ext, mix_ref, tp, first_row, row_count, tokens):
    half = jnp.left_shift(jnp.int32(1), tp)
    reached = ext.shape[0]
    shape = (tokens, reached)
    out_tok = lax.broadcasted_iota(jnp.int32, shape, 0)
    in_tok = lax.broadcasted_iota(jnp.int32, shape, 1)
    row_step = in_tok // GRID_W - REACH - out_tok // GRID_W
    col_step = in_tok % GRID_W - out_tok % GRID_W
    inside = (row_step >= -half) & (row_step < half) & (col_step >= -half) & (col_step < half)
    box = jnp.where(inside, 1.0, 0.0).astype(jnp.bfloat16)
    total = jnp.dot(box, ext[...], preferred_element_type=jnp.float32)
    tok = lax.broadcasted_iota(jnp.int32, (tokens, 1), 0)
    row, col = first_row + tok // GRID_W, tok % GRID_W
    rows = jnp.minimum(row + half, row_count) - jnp.maximum(row - half, 0)
    cols = jnp.minimum(col + half, GRID_W) - jnp.maximum(col - half, 0)
    count = (rows * cols).astype(jnp.float32)
    own = ext[REACH * GRID_W : REACH * GRID_W + tokens].astype(jnp.float32)
    diff = (total / count - own).astype(jnp.bfloat16)
    return jnp.dot(diff, mix_ref[0], preferred_element_type=jnp.float32).astype(jnp.bfloat16)


def gate_stage(wide, taps_ref, rec_ref, ing_ref, rate_ref, logd_ref, keep, drive, tokens):
    tap_count = taps_ref.shape[0]
    taps = taps_ref[...].astype(jnp.float32)
    left = tap_count // 2
    blocks, head = rec_ref.shape[1:3]
    for block in range(blocks):
        lanes = slice(block * head, (block + 1) * head)
        conv = wide[EDGE - left : EDGE - left + tokens, lanes] * taps[0:1, lanes]
        for k in range(1, tap_count):
            at = EDGE - left + k
            conv = conv + wide[at : at + tokens, lanes] * taps[k : k + 1, lanes]
        conv_in = conv.astype(jnp.bfloat16)
        drive_in = conv_in.astype(jnp.float32)
        for d in range(2):
            rec = jax.nn.sigmoid(
                jnp.dot(conv_in, rec_ref[d, block], preferred_element_type=jnp.float32)
            )
            ing = jax.nn.sigmoid(
                jnp.dot(conv_in, ing_ref[d, block], preferred_element_type=jnp.float32)
            )
            log_keep = -8.0 * rec * rate_ref[d : d + 1, lanes] + logd_ref[:, d : d + 1]
            keep[d * blocks + block] = jnp.exp(log_keep)
            drive[d * blocks + block] = jnp.sqrt(one_minus_exp(2.0 * log_keep)) * ing * drive_in


def scan_stage(keep, drive, tokens):
    steps = tokens // CHUNKS
    count, head = keep.shape[0], keep.shape[2]

    def step(i, carry):
        after = []
        for k in range(count):
            at = i if k < count // 2 else steps - 1 - i
            rows = pl.ds(at, CHUNKS, stride=steps)
            a = keep[k, rows, :]
            prod = a * carry[2 * k]
            state = a * carry[2 * k + 1] + drive[k, rows, :]
            keep[k, rows, :] = prod
            drive[k, rows, :] = state
            after += [prod, state]
        return tuple(after)

    one = jnp.ones((CHUNKS, head), jnp.float32)
    zero = jnp.zeros((CHUNKS, head), jnp.float32)
    out = lax.fori_loop(0, steps, step, (one, zero) * count)
    halves = (out[:count], out[count:])
    return tuple(jnp.concatenate(half[j::2], axis=1) for half in halves for j in range(2))


def run_summary(pf, hf, pb, hb):
    fp, fh = pf[0:1], hf[0:1]
    bp, bh = pb[CHUNKS - 1 :], hb[CHUNKS - 1 :]
    for c in range(1, CHUNKS):
        fh = pf[c : c + 1] * fh + hf[c : c + 1]
        fp = fp * pf[c : c + 1]
        r = CHUNKS - 1 - c
        bh = pb[r : r + 1] * bh + hb[r : r + 1]
        bp = bp * pb[r : r + 1]
    return jnp.concatenate([fp, fh, bp, bh], axis=0)


def close_stage(keep, drive, ends, enter_f, enter_b, y_ref, tokens):
    pf, hf, pb, hb = ends
    steps = tokens // CHUNKS
    fs, bs = [enter_f], [enter_b]
    for c in range(CHUNKS - 1):
        fs.append(pf[c : c + 1] * fs[-1] + hf[c : c + 1])
        r = CHUNKS - 1 - c
        bs.append(pb[r : r + 1] * bs[-1] + hb[r : r + 1])
    blocks, head = keep.shape[0] // 2, keep.shape[2]
    for c in range(CHUNKS):
        rows = slice(c * steps, (c + 1) * steps)
        for block in range(blocks):
            lanes = slice(block * head, (block + 1) * head)
            y_ref[rows, lanes] = (
                keep[block, rows, :] * fs[c][:, lanes]
                + drive[block, rows, :]
                + keep[blocks + block, rows, :] * bs[CHUNKS - 1 - c][:, lanes]
                + drive[blocks + block, rows, :]
            ).astype(jnp.bfloat16)


def remote(src, dst, send_sem, recv_sem, axis, index):
    return pltpu.make_async_remote_copy(
        src_ref=src,
        dst_ref=dst,
        send_sem=send_sem,
        recv_sem=recv_sem,
        device_id={axis: index},
        device_id_type=pl.DeviceIdType.MESH,
    )


class BlockGather:
    def __init__(self, buf, sems, me, sp):
        self.buf, self.sems = buf, sems
        self.line = sp // 2
        self.a, self.b = me // 2, me % 2

    def copy(self, origin, other, send, recv, target):
        block = self.buf.at[origin * 2 + other]
        return remote(
            block, block, self.sems.at[send, origin], self.sems.at[recv, origin], "sp", target
        )

    def right(self, o):
        return self.copy(o, self.b, 0, 3, (self.a + 1) * 2 + self.b)

    def left(self, o):
        return self.copy(o, self.b, 1, 3, (self.a - 1) * 2 + self.b)

    def across(self, o):
        return self.copy(o, self.b, 2, 4, self.a * 2 + 1 - self.b)

    def landed(self, o):
        return self.copy(o, 1 - self.b, 2, 4, self.a * 2 + 1 - self.b)

    def start(self):
        a = self.a

        @pl.when(a < self.line - 1)
        def _():
            self.right(a).start()

        @pl.when(a > 0)
        def _():
            self.left(a).start()

        self.across(a).start()

    def step(self, d):
        a, line = self.a, self.line
        low, high = a - d, a + d

        @pl.when(low >= 0)
        def _():
            self.right(low).wait_recv()

            @pl.when(a < line - 1)
            def _():
                self.right(low).start()

            self.across(low).start()

        @pl.when(high < line)
        def _():
            self.left(high).wait_recv()

            @pl.when(a > 0)
            def _():
                self.left(high).start()

            self.across(high).start()

    def both(self, d, use, wait=False, other=None):
        a = self.a
        side = self.b if other is None else other
        for origin, there in ((a - d, a - d >= 0), (a + d, (a + d < self.line) & (d > 0))):

            @pl.when(there)
            def _(origin=origin):
                if wait:
                    self.landed(origin).wait_recv()
                use(origin * 2 + side)

    def finish(self):
        a, line = self.a, self.line

        @pl.loop(0, line)
        def _(o):
            @pl.when((o <= a) & (a < line - 1))
            def _():
                self.right(o).wait_send()

            @pl.when((o >= a) & (a > 0))
            def _():
                self.left(o).wait_send()

            self.across(o).wait_send()


def layer_kernel(
    tok,
    gain,
    wpi,
    wli,
    mix,
    taps,
    rec,
    ing,
    rate,
    logd,
    start,
    wpo,
    wlo,
    out,
    toks,
    normed,
    win,
    wout,
    acc,
    ext,
    edge,
    ulru,
    wide,
    keep,
    drive,
    mine,
    sums,
    y_pool,
    y_lru,
    part,
    red,
    own_sem,
    tok_sem,
    in_sem,
    out_sem,
    halo_sem,
    sum_sem,
    red_sem,
    *,
    sp,
    tp,
):
    f32 = jnp.float32
    me, t = lax.axis_index("sp"), lax.axis_index("tp")
    count, local = tok.shape
    depth, wide_out = wpi.shape[0], wpo.shape[1]
    share = count // tp
    halo = REACH * GRID_W

    owns = [
        pltpu.make_async_copy(src, dst, own_sem.at[k])
        for k, (src, dst) in enumerate(
            (
                (wpi, win.at[me, 0]),
                (wli, win.at[me, 1]),
                (tok, toks.at[t]),
                (wpo, wout.at[me, 0]),
                (wlo, wout.at[me, 1]),
            )
        )
    ]
    for own in owns:
        own.start()

    def tok_copy(k, source, target):
        return remote(tok, toks.at[source], tok_sem.at[0, k], tok_sem.at[1, k], "tp", target)

    for k in range(1, tp):
        tok_copy(k, t, lax.rem(t + k, tp)).start()
    owns[0].wait()
    owns[1].wait()
    first = BlockGather(win, in_sem, me, sp)
    line = first.line
    first.start()
    early = min(3, line)
    for d in range(1, early):
        first.step(d)

    owns[2].wait()
    for k in range(1, tp):
        source = lax.rem(t - k + tp, tp)
        tok_copy(k, source, source).wait_recv()
    square = jnp.zeros((count, 1), f32)
    for p in range(tp):
        v = toks[p].astype(f32)
        square = square + jnp.sum(v * v, axis=1, keepdims=True)
    scale = lax.rsqrt(square / (tp * local) + EPSILON)
    for p in range(tp):
        for q in range(local // depth):
            v = toks[p, :, q * depth : (q + 1) * depth].astype(f32)
            at = p * local + q * depth
            normed[p * (local // depth) + q] = (
                v * scale * gain[:, at : at + depth]
            ).astype(jnp.bfloat16)

    acc[...] = jnp.zeros_like(acc)

    def use_in(block):
        for j in range(2):
            acc[j] += jnp.dot(normed[block], win[block, j], preferred_element_type=f32)

    @pl.loop(0, early)
    def _(d):
        first.both(d, use_in)

    @pl.loop(early, line)
    def _(d):
        first.step(d)
        first.both(d, use_in)

    @pl.loop(0, line)
    def _(d):
        first.both(d, use_in, wait=True, other=1 - first.b)

    ext[halo : halo + count] = acc[0].astype(jnp.bfloat16)
    ulru[...] = acc[1].astype(jnp.bfloat16)

    def to_next(part_of):
        if part_of == 0:
            src, dst = ext.at[pl.ds(count, halo)], ext.at[pl.ds(0, halo)]
        else:
            src, dst = ulru.at[pl.ds(count - EDGE, EDGE)], edge.at[0]
        return remote(src, dst, halo_sem.at[0, part_of], halo_sem.at[1, part_of], "sp", me + 1)

    def to_prev(part_of):
        k = 2 + part_of
        if part_of == 0:
            src, dst = ext.at[pl.ds(halo, halo)], ext.at[pl.ds(halo + count, halo)]
        else:
            src, dst = ulru.at[pl.ds(0, EDGE)], edge.at[1]
        return remote(src, dst, halo_sem.at[0, k], halo_sem.at[1, k], "sp", me - 1)

    for part_of in (1, 0):

        @pl.when(me < sp - 1)
        def _(part_of=part_of):
            to_next(part_of).start()

        @pl.when(me > 0)
        def _(part_of=part_of):
            to_prev(part_of).start()

    owns[3].wait()
    owns[4].wait()
    second = BlockGather(wout, out_sem, me, sp)
    second.start()

    @pl.when(me == 0)
    def _():
        edge[0] = jnp.zeros(edge.shape[1:], edge.dtype)
        ext[0:halo] = jnp.zeros((halo, ext.shape[1]), ext.dtype)

    @pl.when(me == sp - 1)
    def _():
        edge[1] = jnp.zeros(edge.shape[1:], edge.dtype)
        ext[halo + count :] = jnp.zeros((halo, ext.shape[1]), ext.dtype)

    def halo_wait(part_of):
        @pl.when(me > 0)
        def _():
            to_next(part_of).wait_recv()

        @pl.when(me < sp - 1)
        def _():
            to_prev(part_of).wait_recv()

    halo_wait(1)
    wide[0:EDGE] = edge[0].astype(f32)
    wide[EDGE : EDGE + count] = ulru[...].astype(f32)
    wide[EDGE + count :] = edge[1].astype(f32)
    gate_stage(wide, taps, rec, ing, rate, logd, keep, drive, count)
    ends = scan_stage(keep, drive, count)
    mine[0:4] = run_summary(*ends)
    mine[4:8] = jnp.zeros((4, mine.shape[1]), f32)
    sums[me] = mine[...]

    def sum_copy(k, source, target):
        return remote(mine, sums.at[source], sum_sem.at[0, k], sum_sem.at[1, k], "sp", target)

    for k in range(1, sp):
        sum_copy(k, me, lax.rem(me + k, sp)).start()
    halo_wait(0)
    grid_rows = count // GRID_W
    y_pool[...] = pool_stage(ext, mix, t, me * grid_rows, sp * grid_rows, count)
    if line > 1:
        second.step(1)
    for k in range(1, sp):
        source = lax.rem(me - k + sp, sp)
        sum_copy(k, source, source).wait_recv()
    enter_f, enter_b = start[0:1], start[1:2]
    for s in range(sp - 1):
        r = sp - 1 - s
        enter_f = jnp.where(s < me, sums[s, 0:1] * enter_f + sums[s, 1:2], enter_f)
        enter_b = jnp.where(r > me, sums[r, 2:3] * enter_b + sums[r, 3:4], enter_b)
    close_stage(keep, drive, ends, enter_f, enter_b, y_lru, count)

    def red_copy(k, block, target):
        rows = pl.ds(pl.multiple_of(target * share, share), share)
        return remote(
            part.at[block, rows],
            red.at[k, block],
            red_sem.at[0, k, block],
            red_sem.at[1, k, block],
            "tp",
            target,
        )

    def use_out(block):
        part[block] = (
            jnp.dot(y_pool[...], wout[block, 0], preferred_element_type=f32)
            + jnp.dot(y_lru[...], wout[block, 1], preferred_element_type=f32)
        ).astype(jnp.bfloat16)
        for k in range(1, tp):
            red_copy(k, block, lax.rem(t + k, tp)).start()

    ready = min(2, line)

    @pl.loop(0, ready)
    def _(d):
        second.both(d, use_out)

    @pl.loop(ready, line)
    def _(d):
        second.step(d)
        second.both(d, use_out)

    @pl.loop(0, line)
    def _(d):
        second.both(d, use_out, wait=True, other=1 - second.b)

    rows = pl.ds(pl.multiple_of(t * share, share), share)
    for block in range(sp):
        total = part[block, rows, :].astype(f32)
        for k in range(1, tp):
            red_copy(k, block, lax.rem(t + k, tp)).wait_recv()
            total = total + red[k, block].astype(f32)
        out[:, block * wide_out : (block + 1) * wide_out] = total.astype(out.dtype)

    first.finish()
    second.finish()
    for k in range(1, tp):
        tok_copy(k, t, lax.rem(t + k, tp)).wait_send()
    for k in range(1, sp):
        sum_copy(k, me, lax.rem(me + k, sp)).wait_send()
    for part_of in range(2):

        @pl.when(me < sp - 1)
        def _(part_of=part_of):
            to_next(part_of).wait_send()

        @pl.when(me > 0)
        def _(part_of=part_of):
            to_prev(part_of).wait_send()

    @pl.loop(0, sp)
    def _(block):
        for k in range(1, tp):
            red_copy(k, block, lax.rem(t + k, tp)).wait_send()


def per_device(
    sp,
    tp,
    tokens,
    norm_gain,
    w_pool_in,
    w_lru_in,
    pool_mix,
    conv_taps,
    rec_gate,
    in_gate,
    decay_rate,
    log_decay,
    start_state,
    w_out_pool,
    w_out_lru,
):
    count, local = tokens.shape
    depth, width = w_lru_in.shape
    wide_out = w_out_pool.shape[1]
    blocks, head = rec_gate.shape[1:3]
    f32, bf16 = jnp.float32, jnp.bfloat16
    vmem = pl.BlockSpec(memory_space=pltpu.VMEM)
    far = pl.BlockSpec(memory_space=pl.ANY)
    share = count // tp
    dma = pltpu.SemaphoreType.DMA
    return pl.pallas_call(
        functools.partial(layer_kernel, sp=sp, tp=tp),
        out_shape=jax.ShapeDtypeStruct((share, wide_out * sp), bf16),
        in_specs=[far, vmem, far, far] + [vmem] * 7 + [far, far],
        out_specs=vmem,
        scratch_shapes=[
            pltpu.VMEM((tp, count, local), bf16),
            pltpu.VMEM((sp, count, depth), bf16),
            pltpu.VMEM((sp, 2, depth, width), bf16),
            pltpu.VMEM((sp, 2, width, wide_out), bf16),
            pltpu.VMEM((2, count, width), f32),
            pltpu.VMEM((count + 2 * REACH * GRID_W, width), bf16),
            pltpu.VMEM((2, EDGE, width), bf16),
            pltpu.VMEM((count, width), bf16),
            pltpu.VMEM((count + 2 * EDGE, width), f32),
            pltpu.VMEM((2 * blocks, count, head), f32),
            pltpu.VMEM((2 * blocks, count, head), f32),
            pltpu.VMEM((8, width), f32),
            pltpu.VMEM((sp, 8, width), f32),
            pltpu.VMEM((count, width), bf16),
            pltpu.VMEM((count, width), bf16),
            pltpu.VMEM((sp, count, wide_out), bf16),
            pltpu.VMEM((tp, sp, share, wide_out), bf16),
            dma((5,)),
            dma((2, tp)),
            dma((5, sp // 2)),
            dma((5, sp // 2)),
            dma((2, 4)),
            dma((2, sp)),
            dma((2, tp, sp)),
        ],
        compiler_params=pltpu.CompilerParams(
            has_side_effects=True, vmem_limit_bytes=60 * 2**20
        ),
    )(
        tokens,
        norm_gain[None],
        w_pool_in,
        w_lru_in,
        pool_mix,
        conv_taps,
        rec_gate,
        in_gate,
        decay_rate,
        log_decay.T,
        start_state,
        w_out_pool,
        w_out_lru,
    )


def solution(mesh):
    placed = (
        P("sp", "tp"),
        P(),
        P("sp", "tp"),
        P("sp", "tp"),
        P("tp", None, None),
        P(None, "tp"),
        P(None, "tp", None, None),
        P(None, "tp", None, None),
        P(None, "tp"),
        P(None, "sp"),
        P(None, "tp"),
        P("tp", "sp"),
        P("tp", "sp"),
    )
    return jax.shard_map(
        functools.partial(per_device, mesh.shape["sp"], mesh.shape["tp"]),
        mesh=mesh,
        in_specs=placed,
        out_specs=P(("sp", "tp"), None),
        check_vma=False,
    )
```

profile of v0, /device:TPU:3, one launch (start us, length us, event | category | flops | bytes accessed | tf_op | source)
XLA Modules:
  0.0 127.2 jit_solution(6155222129504612430)
XLA Ops:
  0.0 1.5 %copy.14 = f32[2,384]{0,1:T(8,128)} copy(f32[2,384]{1,0:T(2,128)} %param.22) | data formatting | bytes 6144 | tf_op args[9]
  1.5 123.9 %shard_map.127 = bf16[96,2048]{1,0:T(8,128)(2,1)} custom-call(bf16[384,512]{1,0:T(8,128)(2,1)} %tok.1, f32[1,2048]{1,0:T(1,128)} %bitcast.3, bf16[256,512]{1,0:T(8,128)(2,1)} %wpi.1, bf16[256,512]{1,0:T(8,128)(2,1)} %wli.1, bf16[1,512,512]{2,1,0:T(8,128)(2,1)} %mix.1, bf16[4,512]{1,0:T(4,128)(2,1)} %taps.1, bf16[2,4,128,128]{3,2,1,0:T(8,128)(2,1)} %rec.1, ...), custom_call_target="tpu_custom_call" | custom-call | tf_op jit(solution)/shard_map/pallas_call | solution.py:514
  125.4 1.8 %copy.16 = bf16[96,2048]{1,0:T(8,128)(2,1)} copy(bf16[96,2048]{1,0:T(8,128)(2,1)} %shard_map.127) | data formatting | bytes 786432
where the time goes:
time: 127 us
  Pallas kernels  124 us (98%)
  local copies, waits for them, and re-layouts  3.27 us (3%)
    pallas_call x1, Pallas kernels, per_device(): pl.pallas_call(functools.partial(layer_kernel, sp=sp, tp=tp), out_shape=j...  124 us
    unnamed x2, local copies, waits for them, and re-layouts  3.27 us

commit v1 on v0

v1 whole, which is shorter than its diff:
```python
import functools

import jax
import jax.numpy as jnp
from jax import lax
from jax.experimental import pallas as pl
from jax.experimental.pallas import tpu as pltpu
from jax.sharding import PartitionSpec as P

POOL_GROUPS = 4
GRID_W = 32
REACH = 2 ** (POOL_GROUPS - 1)
EPSILON = 1e-06
EDGE = 16
CHUNKS = 8
PIECES = 2


def one_minus_exp(y):
    series = jnp.full_like(y, 1.0 / 40320.0)
    for factorial in (5040.0, 720.0, 120.0, 24.0, 6.0, 2.0, 1.0):
        series = series * y + 1.0 / factorial
    return jnp.where(y > -0.35, -y * series, 1.0 - jnp.exp(y))


def pool_stage(ext, mix_ref, tp, first_row, row_count, tokens):
    half = jnp.left_shift(jnp.int32(1), tp)
    reached = ext.shape[0]
    shape = (tokens, reached)
    out_tok = lax.broadcasted_iota(jnp.int32, shape, 0)
    in_tok = lax.broadcasted_iota(jnp.int32, shape, 1)
    row_step = in_tok // GRID_W - REACH - out_tok // GRID_W
    col_step = in_tok % GRID_W - out_tok % GRID_W
    inside = (row_step >= -half) & (row_step < half) & (col_step >= -half) & (col_step < half)
    box = jnp.where(inside, 1.0, 0.0).astype(jnp.bfloat16)
    total = jnp.dot(box, ext[...], preferred_element_type=jnp.float32)
    tok = lax.broadcasted_iota(jnp.int32, (tokens, 1), 0)
    row, col = first_row + tok // GRID_W, tok % GRID_W
    rows = jnp.minimum(row + half, row_count) - jnp.maximum(row - half, 0)
    cols = jnp.minimum(col + half, GRID_W) - jnp.maximum(col - half, 0)
    count = (rows * cols).astype(jnp.float32)
    own = ext[REACH * GRID_W : REACH * GRID_W + tokens].astype(jnp.float32)
    diff = (total / count - own).astype(jnp.bfloat16)
    return jnp.dot(diff, mix_ref[0], preferred_element_type=jnp.float32).astype(jnp.bfloat16)


def gate_stage(wide, taps_ref, rec_ref, ing_ref, rate_ref, logd, keep, drive, tokens):
    tap_count = taps_ref.shape[0]
    taps = taps_ref[...].astype(jnp.float32)
    left = tap_count // 2
    blocks, head = rec_ref.shape[1:3]
    for block in range(blocks):
        lanes = slice(block * head, (block + 1) * head)
        conv = wide[EDGE - left : EDGE - left + tokens, lanes] * taps[0:1, lanes]
        for k in range(1, tap_count):
            at = EDGE - left + k
            conv = conv + wide[at : at + tokens, lanes] * taps[k : k + 1, lanes]
        conv_in = conv.astype(jnp.bfloat16)
        drive_in = conv_in.astype(jnp.float32)
        for d in range(2):
            rec = jax.nn.sigmoid(
                jnp.dot(conv_in, rec_ref[d, block], preferred_element_type=jnp.float32)
            )
            ing = jax.nn.sigmoid(
                jnp.dot(conv_in, ing_ref[d, block], preferred_element_type=jnp.float32)
            )
            log_keep = -8.0 * rec * rate_ref[d : d + 1, lanes] + logd[:, d : d + 1]
            keep[d * blocks + block] = jnp.exp(log_keep)
            drive[d * blocks + block] = jnp.sqrt(one_minus_exp(2.0 * log_keep)) * ing * drive_in


def scan_stage(keep, drive, tokens):
    steps = tokens // CHUNKS
    count, head = keep.shape[0], keep.shape[2]

    def step(i, carry):
        after = []
        for k in range(count):
            at = i if k < count // 2 else steps - 1 - i
            rows = pl.ds(at, CHUNKS, stride=steps)
            a = keep[k, rows, :]
            prod = a * carry[2 * k]
            state = a * carry[2 * k + 1] + drive[k, rows, :]
            keep[k, rows, :] = prod
            drive[k, rows, :] = state
            after += [prod, state]
        return tuple(after)

    one = jnp.ones((CHUNKS, head), jnp.float32)
    zero = jnp.zeros((CHUNKS, head), jnp.float32)
    out = lax.fori_loop(0, steps, step, (one, zero) * count)
    halves = (out[:count], out[count:])
    return tuple(jnp.concatenate(half[j::2], axis=1) for half in halves for j in range(2))


def run_summary(pf, hf, pb, hb):
    fp, fh = pf[0:1], hf[0:1]
    bp, bh = pb[CHUNKS - 1 :], hb[CHUNKS - 1 :]
    for c in range(1, CHUNKS):
        fh = pf[c : c + 1] * fh + hf[c : c + 1]
        fp = fp * pf[c : c + 1]
        r = CHUNKS - 1 - c
        bh = pb[r : r + 1] * bh + hb[r : r + 1]
        bp = bp * pb[r : r + 1]
    return jnp.concatenate([fp, fh, bp, bh], axis=0)


def close_stage(keep, drive, ends, enter_f, enter_b, y_ref, tokens):
    pf, hf, pb, hb = ends
    steps = tokens // CHUNKS
    fs, bs = [enter_f], [enter_b]
    for c in range(CHUNKS - 1):
        fs.append(pf[c : c + 1] * fs[-1] + hf[c : c + 1])
        r = CHUNKS - 1 - c
        bs.append(pb[r : r + 1] * bs[-1] + hb[r : r + 1])
    blocks, head = keep.shape[0] // 2, keep.shape[2]
    for c in range(CHUNKS):
        rows = slice(c * steps, (c + 1) * steps)
        for block in range(blocks):
            lanes = slice(block * head, (block + 1) * head)
            y_ref[rows, lanes] = (
                keep[block, rows, :] * fs[c][:, lanes]
                + drive[block, rows, :]
                + keep[blocks + block, rows, :] * bs[CHUNKS - 1 - c][:, lanes]
                + drive[blocks + block, rows, :]
            ).astype(jnp.bfloat16)


def remote(src, dst, send_sem, recv_sem, device):
    return pltpu.make_async_remote_copy(
        src_ref=src,
        dst_ref=dst,
        send_sem=send_sem,
        recv_sem=recv_sem,
        device_id=device,
        device_id_type=pl.DeviceIdType.MESH,
    )


class Place:
    def __init__(self, sp, tp):
        me, t = lax.axis_index("sp"), lax.axis_index("tp")
        self.sp, self.tp, self.me, self.t = sp, tp, me, t
        self.lines, self.cols = sp // 2, tp // 2
        self.line, self.side = me // 2, me % 2
        self.col, self.core = t // 2, t % 2
        self.low = self.line % 2
        self.mate = self.line + 1 - 2 * self.low
        self.home = self.core == self.low
        self.run = (self.line // 2 * 2 + self.core) * 2 + self.side
        self.part = self.col * 2 + self.low

    def at(self, line=None, side=None, col=None, core=None):
        line = self.line if line is None else line
        side = self.side if side is None else side
        col = self.col if col is None else col
        core = self.core if core is None else core
        return {"sp": line * 2 + side, "tp": col * 2 + core}

    def sibling(self):
        return self.at(core=1 - self.core)

    def of_run(self, run):
        return self.at(line=run // 4 * 2 + self.low, side=run % 2, core=run // 2 % 2)


class Spread:
    def __init__(self, place, srcs, buf, own, src_sem, sib_sem, line_sem, pass_sem, recv):
        self.pos, self.srcs, self.buf, self.own = place, srcs, buf, own
        self.src_sem, self.sib_sem, self.line_sem = src_sem, sib_sem, line_sem
        self.pass_sem, self.recv = pass_sem, recv
        self.rows = buf.shape[2] // PIECES

    def piece(self, o, j, p):
        return self.buf.at[o, j, pl.ds(p * self.rows, self.rows)]

    def load_copy(self, j):
        return pltpu.make_async_copy(self.srcs[j], self.buf.at[self.pos.me, j], self.own.at[j])

    def load(self):
        @pl.when(self.pos.home)
        def _():
            for j in range(2):
                self.load_copy(j).start()

    def loaded(self):
        @pl.when(self.pos.home)
        def _():
            for j in range(2):
                self.load_copy(j).wait()

    def source_copy(self, j, p, way):
        pos = self.pos
        return remote(
            self.srcs[j].at[pl.ds(p * self.rows, self.rows)],
            self.piece(pos.me, j, p),
            self.src_sem.at[way, j, p],
            self.recv.at[pos.me, j, p],
            pos.at(line=pos.line + 1 - 2 * way, core=j),
        )

    def source(self, act):
        pos = self.pos
        for way, there in ((0, pos.line + 1 < pos.lines), (1, pos.line > 0)):

            @pl.when(jnp.logical_not(pos.home) & there)
            def _(way=way):
                for p in range(PIECES):
                    for j in range(2):
                        act(self.source_copy(j, p, way))

    def share_copy(self, j, p):
        pos = self.pos
        piece = self.piece(pos.me, j, p)
        return remote(
            piece, piece, self.sib_sem.at[j, p], self.recv.at[pos.me, j, p], pos.sibling()
        )

    def share(self, act):
        @pl.when(self.pos.home)
        def _():
            for p in range(PIECES):
                for j in (1 - self.pos.core, self.pos.core):
                    act(self.share_copy(j, p))

    def block(self, line, p, kind, device):
        pos = self.pos
        o = line * 2 + pos.side
        piece = self.piece(o, pos.core, p)
        return remote(
            piece, piece, self.line_sem.at[kind, line, p], self.recv.at[o, pos.core, p], device
        )

    def to_line(self, line, p, act):
        pos = self.pos

        @pl.when((line <= pos.line) & (pos.line + 2 < pos.lines))
        def _():
            act(self.block(line, p, 0, pos.at(line=pos.line + 2)))

        @pl.when((line >= pos.line) & (pos.line >= 2))
        def _():
            act(self.block(line, p, 1, pos.at(line=pos.line - 2)))

    def to_side(self, line, p, act):
        act(self.block(line, p, 2, self.pos.at(side=1 - self.pos.side)))

    def to_sibling(self, o, p, act):
        piece = self.piece(o, self.pos.core, p)
        act(
            remote(
                piece,
                piece,
                self.pass_sem.at[o, p],
                self.recv.at[o, self.pos.core, p],
                self.pos.sibling(),
            )
        )

    def await_piece(self, o, j, p):
        piece = self.piece(o, j, p)
        remote(
            piece, piece, self.pass_sem.at[o, p], self.recv.at[o, j, p], self.pos.sibling()
        ).wait_recv()

    def around(self, d, act):
        pos = self.pos
        for line, there in (
            (pos.line - d, pos.line - d >= 0),
            (pos.line + d, (pos.line + d < pos.lines) & (d > 0)),
        ):

            @pl.when(there)
            def _(line=line):
                act(line)

    def first(self, line=True, side=True, wait=True):
        pos = self.pos
        for p in range(PIECES):
            if wait:

                @pl.when(jnp.logical_not(pos.home))
                def _(p=p):
                    self.await_piece(pos.me, pos.core, p)

            if side:
                self.to_side(pos.line, p, lambda copy: copy.start())
            if line:
                self.to_line(pos.line, p, lambda copy: copy.start())

    def relay(self, d):
        def act(line):
            o = line * 2 + self.pos.side
            for p in range(PIECES):
                self.await_piece(o, self.pos.core, p)
                self.to_line(line, p, lambda copy: copy.start())
                self.to_side(line, p, lambda copy: copy.start())
                self.to_sibling(o, p, lambda copy: copy.start())

        self.around(d, act)

    def crossed(self, d):
        def act(line):
            o = line * 2 + 1 - self.pos.side
            for p in range(PIECES):
                self.await_piece(o, self.pos.core, p)
                self.to_sibling(o, p, lambda copy: copy.start())

        self.around(d, act)

    def use(self, d, act):
        pos = self.pos

        def both(line):
            for other in range(2):
                o = line * 2 + (pos.side if other == 0 else 1 - pos.side)

                @pl.when(jnp.logical_not((o == pos.me) & pos.home))
                def _():
                    for p in range(PIECES):
                        self.await_piece(o, 1 - pos.core, p)

                act(o)

        self.around(d, both)

    def finish(self):
        pos = self.pos
        done = lambda copy: copy.wait_send()
        self.source(done)
        self.share(done)

        @pl.loop(0, pos.lines)
        def _(line):
            for p in range(PIECES):
                self.to_line(line, p, done)
                self.to_side(line, p, done)

                @pl.when(line != pos.line)
                def _():
                    self.to_sibling(line * 2 + pos.side, p, done)

                self.to_sibling(line * 2 + 1 - pos.side, p, done)


def layer_kernel(
    tok,
    gain,
    wpi,
    wli,
    mix_in,
    taps_in,
    rec_in,
    ing_in,
    rate_in,
    logd_in,
    start_in,
    wpo,
    wlo,
    out,
    toks,
    normed,
    win,
    wout,
    acc,
    ext,
    edge,
    ulru,
    wide,
    keep,
    drive,
    mine,
    sums,
    y_pool,
    y_lru,
    part,
    cross,
    half_sum,
    last,
    mix,
    taps,
    rec,
    ing,
    rate,
    logd,
    start,
    par_sem,
    tok_own,
    tok_send,
    tok_pass,
    tok_recv,
    in_own,
    in_src,
    in_sib,
    in_line,
    in_pass,
    in_recv,
    out_own,
    out_src,
    out_sib,
    out_line,
    out_pass,
    out_recv,
    halo_sem,
    sum_sem,
    cross_sem,
    last_sem,
    *,
    sp,
    tp,
):
    f32 = jnp.float32
    begin = lambda copy: copy.start()
    pos = Place(sp, tp)
    run, group, line, core, home = pos.run, pos.part, pos.line, pos.core, pos.home
    away = jnp.logical_not(home)
    count, local = tok.shape
    depth, wide_out = wpi.shape[0], wpo.shape[1]
    share = count // tp
    halo = REACH * GRID_W
    lines, cols = pos.lines, pos.cols

    weights_in = Spread(
        pos, (wpi, wli), win, in_own, in_src, in_sib, in_line, in_pass, in_recv
    )
    weights_out = Spread(
        pos, (wpo, wlo), wout, out_own, out_src, out_sib, out_line, out_pass, out_recv
    )
    weights_in.load()
    weights_out.load()

    def tok_local():
        return pltpu.make_async_copy(tok, toks.at[pos.t], tok_own.at[0])

    def tok_copy(k, device):
        return remote(tok, toks.at[pos.t], tok_send.at[k], tok_recv.at[pos.t], device)

    def tok_sends(act):
        act(tok_copy(0, pos.at(line=pos.mate, core=pos.low)))
        for k in range(1, cols):
            act(tok_copy(k, pos.at(col=lax.rem(pos.col + k, cols), core=pos.low)))

        @pl.when(away)
        def _():
            act(tok_copy(cols, pos.sibling()))

    def tok_relay(k, c, act):
        f = pos.col * 2 + c
        act(
            remote(
                toks.at[f],
                toks.at[f],
                tok_pass.at[k, c],
                tok_recv.at[f],
                pos.at(col=lax.rem(pos.col + k, cols)),
            )
        )

    def tok_wait(f):
        remote(toks.at[f], toks.at[f], tok_send.at[0], tok_recv.at[f], pos.sibling()).wait_recv()

    params = ((mix_in, mix), (rec_in, rec), (ing_in, ing))
    smalls = ((taps_in, taps), (rate_in, rate), (start_in, start))

    def param_sends(act):
        @pl.when(home)
        def _():
            for k, (src, dst) in enumerate(params + smalls):
                act(remote(src, dst, par_sem.at[0, k], par_sem.at[1, k], pos.sibling()))
            k = len(params + smalls)
            act(remote(logd_in, logd, par_sem.at[0, k], par_sem.at[1, k], pos.at(line=pos.mate)))

    def param_locals():
        return [
            pltpu.make_async_copy(src, dst, par_sem.at[1, k])
            for k, (src, dst) in enumerate(params)
        ]

    tok_sends(begin)

    @pl.when(home)
    def _():
        tok_local().start()

    weights_in.source(begin)
    weights_in.loaded()
    weights_in.share(begin)
    weights_in.first()
    param_sends(begin)

    @pl.when(home)
    def _():
        for copy in param_locals():
            copy.start()
        for src, dst in smalls + ((logd_in, logd),):
            dst[...] = src[...]

    weights_out.loaded()
    weights_out.share(begin)
    weights_out.first(line=False)

    for g in range(tp):

        @pl.when(group == g)
        def _(g=g):
            above, below = 2**g * GRID_W, (2**g - 1) * GRID_W
            if above < halo:
                ext[0 : halo - above] = jnp.zeros((halo - above, ext.shape[1]), ext.dtype)
            ext[halo + count + below :] = jnp.zeros((halo - below, ext.shape[1]), ext.dtype)

            @pl.when(run == 0)
            def _():
                ext[halo - above : halo] = jnp.zeros((above, ext.shape[1]), ext.dtype)

            if below > 0:

                @pl.when(run == sp - 1)
                def _():
                    ext[halo + count : halo + count + below] = jnp.zeros(
                        (below, ext.shape[1]), ext.dtype
                    )

    @pl.when(run == 0)
    def _():
        edge[0] = jnp.zeros(edge.shape[1:], edge.dtype)

    @pl.when(run == sp - 1)
    def _():
        edge[1] = jnp.zeros(edge.shape[1:], edge.dtype)

    acc[...] = jnp.zeros_like(acc)

    @pl.when(away)
    def _():
        for c in range(2):
            tok_wait(pos.col * 2 + c)
            for k in range(1, cols):
                tok_relay(k, c, begin)

    weights_in.relay(1)
    weights_in.crossed(0)

    @pl.loop(2, lines)
    def _(d):
        weights_in.relay(d)
        weights_in.crossed(d - 1)

    weights_out.source(begin)
    weights_out.first(side=False, wait=False)

    @pl.when(home)
    def _():
        tok_local().wait()
        tok_wait(pos.col * 2 + 1 - core)

    for k in range(1, cols):
        for c in range(2):
            tok_wait(lax.rem(pos.col + k, cols) * 2 + c)
    square = jnp.zeros((count, 1), f32)
    for p in range(tp):
        v = toks[p].astype(f32)
        square = square + jnp.sum(v * v, axis=1, keepdims=True)
    scale = lax.rsqrt(square / (tp * local) + EPSILON)
    for p in range(tp):
        for q in range(local // depth):
            v = toks[p, :, q * depth : (q + 1) * depth].astype(f32)
            at = p * local + q * depth
            normed[p * (local // depth) + q] = (
                v * scale * gain[:, at : at + depth]
            ).astype(jnp.bfloat16)

    def use_in(block):
        for j in range(2):
            acc[j] += jnp.dot(normed[block], win[block, j], preferred_element_type=f32)

    @pl.loop(0, lines - 1)
    def _(d):
        weights_in.use(d, use_in)

    weights_in.crossed(lines - 1)
    weights_in.use(lines - 1, use_in)

    ext[halo : halo + count] = acc[0].astype(jnp.bfloat16)
    ulru[...] = acc[1].astype(jnp.bfloat16)

    def edge_copy(k):
        if k == 0:
            src, dst, device = ulru.at[pl.ds(count - EDGE, EDGE)], edge.at[0], pos.of_run(run + 1)
        else:
            src, dst, device = ulru.at[pl.ds(0, EDGE)], edge.at[1], pos.of_run(run - 1)
        return remote(src, dst, halo_sem.at[0, k], halo_sem.at[1, k], device)

    def halo_copy(k, g):
        above, below = 2**g * GRID_W, (2**g - 1) * GRID_W
        if k == 0:
            src = ext.at[pl.ds(halo + count - above, above)]
            dst, device = ext.at[pl.ds(halo - above, above)], pos.of_run(run + 1)
        else:
            src = ext.at[pl.ds(halo, below)]
            dst, device = ext.at[pl.ds(halo + count, below)], pos.of_run(run - 1)
        return remote(src, dst, halo_sem.at[0, 2 + k], halo_sem.at[1, 2 + k], device)

    def edges(act, flip=False):
        for k, there in enumerate((run < sp - 1, run > 0)):
            if flip:
                there = (run > 0, run < sp - 1)[k]

            @pl.when(there)
            def _(k=k):
                act(edge_copy(k))

    def halos(act, flip=False):
        for g in range(tp):
            for k, there in enumerate((run < sp - 1, run > 0)):
                if flip:
                    there = (run > 0, run < sp - 1)[k]
                if k == 1 and g == 0:
                    continue

                @pl.when(there & (group == g))
                def _(k=k, g=g):
                    act(halo_copy(k, g))

    edges(begin)
    halos(begin)

    @pl.when(home)
    def _():
        for copy in param_locals():
            copy.wait()

    @pl.when(away)
    def _():
        for k, (_src, dst) in enumerate(params + smalls + ((logd_in, logd),)):
            remote(
                dst, dst, par_sem.at[0, k], par_sem.at[1, k], pos.sibling()
            ).wait_recv()

    weights_out.relay(1)
    weights_out.crossed(0)
    edges(lambda copy: copy.wait_recv(), flip=True)
    wide[0:EDGE] = edge[0].astype(f32)
    wide[EDGE : EDGE + count] = ulru[...].astype(f32)
    wide[EDGE + count :] = edge[1].astype(f32)
    pad = jnp.zeros((8 - logd.shape[0], count), f32)
    decay = jnp.transpose(jnp.concatenate([logd[...], pad], axis=0))
    gate_stage(wide, taps, rec, ing, rate, decay, keep, drive, count)
    if lines > 2:
        weights_out.relay(2)
        weights_out.crossed(1)
    ends = scan_stage(keep, drive, count)
    mine[0:4] = run_summary(*ends)
    mine[4:8] = jnp.zeros((4, mine.shape[1]), f32)
    sums[run] = mine[...]

    def sum_copy(k, source, target):
        return remote(
            mine, sums.at[source], sum_sem.at[0, k], sum_sem.at[1, k], pos.of_run(target)
        )

    for k in range(1, sp):
        sum_copy(k, run, lax.rem(run + k, sp)).start()
    halos(lambda copy: copy.wait_recv(), flip=True)
    grid_rows = count // GRID_W
    y_pool[...] = pool_stage(ext, mix, group, run * grid_rows, sp * grid_rows, count)
    for k in range(1, sp):
        source = lax.rem(run - k + sp, sp)
        sum_copy(k, source, source).wait_recv()
    enter_f, enter_b = start[0:1], start[1:2]
    for s in range(sp - 1):
        r = sp - 1 - s
        enter_f = jnp.where(s < run, sums[s, 0:1] * enter_f + sums[s, 1:2], enter_f)
        enter_b = jnp.where(r > run, sums[r, 2:3] * enter_b + sums[r, 3:4], enter_b)
    close_stage(keep, drive, ends, enter_f, enter_b, y_lru, count)

    pair = 2 * share

    def cross_copy(k, block):
        col = lax.rem(pos.col + k, cols)
        rows = pl.ds(pl.multiple_of(col * pair, pair), pair)
        return remote(
            part.at[block, rows],
            cross.at[k - 1, block],
            cross_sem.at[0, k - 1, block],
            cross_sem.at[1, k - 1, block],
            pos.at(col=col),
        )

    def last_copy(c, block, device):
        return remote(
            half_sum.at[block, pl.ds(c * share, share)],
            last.at[1, block],
            last_sem.at[c, block],
            last_sem.at[2, block],
            device,
        )

    def last_near(block):
        rows = pl.ds(pl.multiple_of((1 - core) * share, share), share)
        return remote(
            half_sum.at[block, rows],
            last.at[0, block],
            last_sem.at[0, block],
            last_sem.at[3, block],
            pos.sibling(),
        )

    def last_sends(block, act):
        @pl.when(home)
        def _():
            act(last_near(block))

        @pl.when(away)
        def _():
            for c in range(2):
                act(last_copy(c, block, pos.at(line=pos.mate, core=c)))

    def use_out(block):
        part[block] = (
            jnp.dot(y_pool[...], wout[block, 0], preferred_element_type=f32)
            + jnp.dot(y_lru[...], wout[block, 1], preferred_element_type=f32)
        ).astype(jnp.bfloat16)
        for k in range(1, cols):
            cross_copy(k, block).start()

    def add_half(block):
        rows = pl.ds(pl.multiple_of(pos.col * pair, pair), pair)
        total = part[block, rows, :].astype(f32)
        for k in range(1, cols):
            cross_copy(k, block).wait_recv()
            total = total + cross[k - 1, block].astype(f32)
        half_sum[block] = total.astype(jnp.bfloat16)
        last_sends(block, begin)

        @pl.when(home)
        def _():
            mine_rows = pl.ds(pl.multiple_of(core * share, share), share)
            last[0, block] = half_sum[block, mine_rows, :]

    def collect(d):
        def both(at):
            add_half(at * 2 + pos.side)
            add_half(at * 2 + 1 - pos.side)

        weights_out.around(d, both)

    weights_out.use(0, use_out)

    @pl.loop(min(3, lines), lines)
    def _(d):
        weights_out.relay(d)
        weights_out.crossed(d - 1)

    @pl.loop(1, lines - 1)
    def _(d):
        weights_out.use(d, use_out)
        collect(d - 1)

    weights_out.crossed(lines - 1)
    weights_out.use(lines - 1, use_out)
    collect(lines - 2)
    collect(lines - 1)

    for block in range(sp):

        @pl.when(away)
        def _(block=block):
            last_near(block).wait_recv()

        last_copy(0, block, pos.sibling()).wait_recv()
        total = last[0, block].astype(f32) + last[1, block].astype(f32)
        out[:, block * wide_out : (block + 1) * wide_out] = total.astype(out.dtype)

    done = lambda copy: copy.wait_send()
    tok_sends(done)
    param_sends(done)

    @pl.when(away)
    def _():
        for c in range(2):
            for k in range(1, cols):
                tok_relay(k, c, done)

    weights_in.finish()
    weights_out.finish()
    edges(done)
    halos(done)
    for k in range(1, sp):
        sum_copy(k, run, lax.rem(run + k, sp)).wait_send()

    @pl.loop(0, sp)
    def _(block):
        for k in range(1, cols):
            cross_copy(k, block).wait_send()
        last_sends(block, done)


def per_device(sp, tp, *args):
    (tokens, norm_gain, w_pool_in, w_lru_in, pool_mix, conv_taps, rec_gate, in_gate) = args[:8]
    (decay_rate, log_decay, start_state, w_out_pool, w_out_lru) = args[8:]
    count, local = tokens.shape
    depth, width = w_lru_in.shape
    wide_out = w_out_pool.shape[1]
    blocks, head = rec_gate.shape[1:3]
    f32, bf16 = jnp.float32, jnp.bfloat16
    vmem = pl.BlockSpec(memory_space=pltpu.VMEM)
    far = pl.BlockSpec(memory_space=pl.ANY)
    share, lines, cols = count // tp, sp // 2, tp // 2
    dma = pltpu.SemaphoreType.DMA
    spread = [
        dma((2,)),
        dma((2, 2, PIECES)),
        dma((2, PIECES)),
        dma((3, lines, PIECES)),
        dma((sp, PIECES)),
        dma((sp, 2, PIECES)),
    ]
    return pl.pallas_call(
        functools.partial(layer_kernel, sp=sp, tp=tp),
        out_shape=jax.ShapeDtypeStruct((share, wide_out * sp), bf16),
        in_specs=[far, vmem, far, far, far, vmem, far, far, vmem, vmem, vmem, far, far],
        out_specs=vmem,
        scratch_shapes=[
            pltpu.VMEM((tp, count, local), bf16),
            pltpu.VMEM((sp, count, depth), bf16),
            pltpu.VMEM((sp, 2, depth, width), bf16),
            pltpu.VMEM((sp, 2, width, wide_out), bf16),
            pltpu.VMEM((2, count, width), f32),
            pltpu.VMEM((count + 2 * REACH * GRID_W, width), bf16),
            pltpu.VMEM((2, EDGE, width), bf16),
            pltpu.VMEM((count, width), bf16),
            pltpu.VMEM((count + 2 * EDGE, width), f32),
            pltpu.VMEM((2 * blocks, count, head), f32),
            pltpu.VMEM((2 * blocks, count, head), f32),
            pltpu.VMEM((8, width), f32),
            pltpu.VMEM((sp, 8, width), f32),
            pltpu.VMEM((count, width), bf16),
            pltpu.VMEM((count, width), bf16),
            pltpu.VMEM((sp, count, wide_out), bf16),
            pltpu.VMEM((cols - 1, sp, 2 * share, wide_out), bf16),
            pltpu.VMEM((sp, 2 * share, wide_out), bf16),
            pltpu.VMEM((2, sp, share, wide_out), bf16),
            pltpu.VMEM(pool_mix.shape, bf16),
            pltpu.VMEM(conv_taps.shape, bf16),
            pltpu.VMEM(rec_gate.shape, bf16),
            pltpu.VMEM(in_gate.shape, bf16),
            pltpu.VMEM(decay_rate.shape, f32),
            pltpu.VMEM(log_decay.shape, f32),
            pltpu.VMEM(start_state.shape, f32),
            dma((2, 7)),
            dma((1,)),
            dma((cols + 1,)),
            dma((cols, 2)),
            dma((tp,)),
        ]
        + spread
        + spread
        + [
            dma((2, 4)),
            dma((2, sp)),
            dma((2, cols - 1, sp)),
            dma((4, sp)),
        ],
        compiler_params=pltpu.CompilerParams(
            has_side_effects=True, vmem_limit_bytes=60 * 2**20
        ),
    )(
        tokens,
        norm_gain[None],
        w_pool_in,
        w_lru_in,
        pool_mix,
        conv_taps,
        rec_gate,
        in_gate,
        decay_rate,
        log_decay,
        start_state,
        w_out_pool,
        w_out_lru,
    )


def solution(mesh):
    placed = (
        P("sp", "tp"),
        P(),
        P("sp", "tp"),
        P("sp", "tp"),
        P("tp", None, None),
        P(None, "tp"),
        P(None, "tp", None, None),
        P(None, "tp", None, None),
        P(None, "tp"),
        P(None, "sp"),
        P(None, "tp"),
        P("tp", "sp"),
        P("tp", "sp"),
    )
    return jax.shard_map(
        functools.partial(per_device, mesh.shape["sp"], mesh.shape["tp"]),
        mesh=mesh,
        in_specs=placed,
        out_specs=P(("sp", "tp"), None),
        check_vma=False,
    )
```

time: 127 us -> 108 us (0.85); the launches traced: 127 us -> 107 us
  Pallas kernels: 124 us -> 105 us
  local copies, waits for them, and re-layouts: 3.27 us -> 1.77 us
    pallas_call x1, Pallas kernels: 124 us -> 105 us  [per_device(): pl.pallas_call(functools.partial(layer_kernel, sp=sp, tp=tp), out_shape=j...]
    unnamed x2 -> x1, local copies, waits for them, and re-layouts: 3.27 us -> 1.77 us
where the time goes in v1:
time: 108 us; the launch traced here: 107 us
  Pallas kernels  105 us (97%)
  local copies, waits for them, and re-layouts  1.77 us (2%)
    pallas_call x1, Pallas kernels, per_device(): pl.pallas_call(functools.partial(layer_kernel, sp=sp, tp=tp), out_shape=j...  105 us

profile of v1, /device:TPU:3, one launch (start us, length us, event | category | flops | bytes accessed | tf_op | source)
XLA Modules:
  0.0 106.5 jit_solution(3999166521501151655)
XLA Ops:
  0.0 104.7 %shard_map.127 = bf16[96,2048]{1,0:T(8,128)(2,1)} custom-call(bf16[384,512]{1,0:T(8,128)(2,1)} %tok.1, f32[1,2048]{1,0:T(1,128)} %bitcast.1, bf16[256,512]{1,0:T(8,128)(2,1)} %wpi.1, bf16[256,512]{1,0:T(8,128)(2,1)} %wli.1, bf16[1,512,512]{2,1,0:T(8,128)(2,1)} %mix_in.1, bf16[4,512]{1,0:T(4,128)(2,1)} %taps_in.1, bf16[2,4,128,128]{3,2,1,0:T(8,128)(2,1)} %rec_in.1, ...), custom_call_target="tpu_custom_call" | custom-call | tf_op jit(solution)/shard_map/pallas_call | solution.py:818
  104.7 1.8 %copy.15 = bf16[96,2048]{1,0:T(8,128)(2,1)} copy(bf16[96,2048]{1,0:T(8,128)(2,1)} %shard_map.127) | data formatting | bytes 786432

commit v2 on v1

--- a/solution.py
+++ b/solution.py
@@ -13,7 +13,8 @@
 EPSILON = 1e-06
 EDGE = 16
 CHUNKS = 8
-PIECES = 2
+PIECES = 4
+TOK_PIECES = 4
 
 
 def one_minus_exp(y):
@@ -44,12 +45,12 @@
     return jnp.dot(diff, mix_ref[0], preferred_element_type=jnp.float32).astype(jnp.bfloat16)
 
 
-def gate_stage(wide, taps_ref, rec_ref, ing_ref, rate_ref, logd, keep, drive, tokens):
+def gate_stage(wide, taps_ref, rec_ref, ing_ref, rate_ref, logd, keep, drive, tokens, some):
     tap_count = taps_ref.shape[0]
     taps = taps_ref[...].astype(jnp.float32)
     left = tap_count // 2
     blocks, head = rec_ref.shape[1:3]
-    for block in range(blocks):
+    for block in some:
         lanes = slice(block * head, (block + 1) * head)
         conv = wide[EDGE - left : EDGE - left + tokens, lanes] * taps[0:1, lanes]
         for k in range(1, tap_count):
@@ -145,7 +146,9 @@
         self.line, self.side = me // 2, me % 2
         self.col, self.core = t // 2, t % 2
         self.low = self.line % 2
-        self.mate = self.line + 1 - 2 * self.low
+        self.toward = 1 - 2 * self.low
+        self.mate = self.line + self.toward
+        self.outer = (self.line == 0) | (self.line == self.lines - 1)
         self.home = self.core == self.low
         self.run = (self.line // 2 * 2 + self.core) * 2 + self.side
         self.part = self.col * 2 + self.low
@@ -165,8 +168,9 @@
 
 
 class Spread:
-    def __init__(self, place, srcs, buf, own, src_sem, sib_sem, line_sem, pass_sem, recv):
+    def __init__(self, place, srcs, buf, stage, own, stage_sem, src_sem, sib_sem, line_sem, pass_sem, recv):
         self.pos, self.srcs, self.buf, self.own = place, srcs, buf, own
+        self.stage, self.stage_sem = stage, stage_sem
         self.src_sem, self.sib_sem, self.line_sem = src_sem, sib_sem, line_sem
         self.pass_sem, self.recv = pass_sem, recv
         self.rows = buf.shape[2] // PIECES
@@ -189,25 +193,56 @@
             for j in range(2):
                 self.load_copy(j).wait()
 
-    def source_copy(self, j, p, way):
+    def rows_of(self, ref, p):
+        return ref.at[pl.ds(p * self.rows, self.rows)]
+
+    def stage_copy(self, j, p):
+        return remote(
+            self.rows_of(self.srcs[j], p),
+            self.rows_of(self.stage, p),
+            self.stage_sem.at[0, p],
+            self.stage_sem.at[1, p],
+            self.pos.sibling(),
+        )
+
+    def staging(self, act):
+        pos = self.pos
+        for j in range(2):
+
+            @pl.when(jnp.logical_not(pos.home) & (pos.core != j))
+            def _(j=j):
+                for p in range(PIECES):
+                    act(self.stage_copy(j, p))
+
+    def source_copy(self, src, p, way):
         pos = self.pos
         return remote(
-            self.srcs[j].at[pl.ds(p * self.rows, self.rows)],
-            self.piece(pos.me, j, p),
-            self.src_sem.at[way, j, p],
-            self.recv.at[pos.me, j, p],
-            pos.at(line=pos.line + 1 - 2 * way, core=j),
-        )
-
-    def source(self, act):
+            self.rows_of(src, p),
+            self.piece(pos.me, pos.core, p),
+            self.src_sem.at[way, p],
+            self.recv.at[pos.me, pos.core, p],
+            pos.at(line=pos.line + pos.toward * (1 - 2 * way)),
+        )
+
+    def source(self, act, wait=False):
         pos = self.pos
-        for way, there in ((0, pos.line + 1 < pos.lines), (1, pos.line > 0)):
-
-            @pl.when(jnp.logical_not(pos.home) & there)
-            def _(way=way):
-                for p in range(PIECES):
-                    for j in range(2):
-                        act(self.source_copy(j, p, way))
+        for p in range(PIECES):
+            if wait:
+
+                @pl.when(pos.home)
+                def _(p=p):
+                    self.stage_copy(0, p).wait_recv()
+
+            for way, there in ((0, True), (1, jnp.logical_not(pos.outer))):
+                for src, mine in (
+                    (self.stage, pos.home),
+                    (self.srcs[0], jnp.logical_not(pos.home) & (pos.core == 0)),
+                    (self.srcs[1], jnp.logical_not(pos.home) & (pos.core == 1)),
+                ):
+
+                    @pl.when(mine & there)
+                    def _(src=src, p=p, way=way):
+                        act(self.source_copy(src, p, way))
 
     def share_copy(self, j, p):
         pos = self.pos
@@ -265,9 +300,10 @@
 
     def around(self, d, act):
         pos = self.pos
+        near, far = pos.line + pos.toward * d, pos.line - pos.toward * d
         for line, there in (
-            (pos.line - d, pos.line - d >= 0),
-            (pos.line + d, (pos.line + d < pos.lines) & (d > 0)),
+            (near, (near >= 0) & (near < pos.lines)),
+            (far, (far >= 0) & (far < pos.lines) & (d > 0)),
         ):
 
             @pl.when(there)
@@ -288,16 +324,20 @@
             if line:
                 self.to_line(pos.line, p, lambda copy: copy.start())
 
-    def relay(self, d):
-        def act(line):
-            o = line * 2 + self.pos.side
-            for p in range(PIECES):
-                self.await_piece(o, self.pos.core, p)
-                self.to_line(line, p, lambda copy: copy.start())
-                self.to_side(line, p, lambda copy: copy.start())
-                self.to_sibling(o, p, lambda copy: copy.start())
-
-        self.around(d, act)
+    def relay(self, d, pieces=range(PIECES), line=True, side=True):
+        for p in pieces:
+
+            def act(at, p=p):
+                o = at * 2 + self.pos.side
+                if line:
+                    self.await_piece(o, self.pos.core, p)
+                    self.to_line(at, p, lambda copy: copy.start())
+                if side:
+                    self.to_side(at, p, lambda copy: copy.start())
+                if line:
+                    self.to_sibling(o, p, lambda copy: copy.start())
+
+            self.around(d, act)
 
     def crossed(self, d):
         def act(line):
@@ -308,11 +348,11 @@
 
         self.around(d, act)
 
-    def use(self, d, act):
+    def use(self, d, act, others=(0, 1)):
         pos = self.pos
 
         def both(line):
-            for other in range(2):
+            for other in others:
                 o = line * 2 + (pos.side if other == 0 else 1 - pos.side)
 
                 @pl.when(jnp.logical_not((o == pos.me) & pos.home))
@@ -327,6 +367,7 @@
     def finish(self):
         pos = self.pos
         done = lambda copy: copy.wait_send()
+        self.staging(done)
         self.source(done)
         self.share(done)
 
@@ -375,7 +416,7 @@
     y_lru,
     part,
     cross,
-    half_sum,
+    joined,
     last,
     mix,
     taps,
@@ -384,18 +425,22 @@
     rate,
     logd,
     start,
+    in_stage,
+    out_stage,
     par_sem,
     tok_own,
     tok_send,
     tok_pass,
     tok_recv,
     in_own,
+    in_stg,
     in_src,
     in_sib,
     in_line,
     in_pass,
     in_recv,
     out_own,
+    out_stg,
     out_src,
     out_sib,
     out_line,
@@ -405,6 +450,7 @@
     sum_sem,
     cross_sem,
     last_sem,
+    mate_sem,
     *,
     sp,
     tp,
@@ -421,10 +467,10 @@
     lines, cols = pos.lines, pos.cols
 
     weights_in = Spread(
-        pos, (wpi, wli), win, in_own, in_src, in_sib, in_line, in_pass, in_recv
+        pos, (wpi, wli), win, in_stage, in_own, in_stg, in_src, in_sib, in_line, in_pass, in_recv
     )
     weights_out = Spread(
-        pos, (wpo, wlo), wout, out_own, out_src, out_sib, out_line, out_pass, out_recv
+        pos, (wpo, wlo), wout, out_stage, out_own, out_stg, out_src, out_sib, out_line, out_pass, out_recv
     )
     weights_in.load()
     weights_out.load()
@@ -432,32 +478,49 @@
     def tok_local():
         return pltpu.make_async_copy(tok, toks.at[pos.t], tok_own.at[0])
 
-    def tok_copy(k, device):
-        return remote(tok, toks.at[pos.t], tok_send.at[k], tok_recv.at[pos.t], device)
+    tok_rows = count // TOK_PIECES
+
+    def tok_piece(ref, n):
+        return ref.at[pl.ds(n * tok_rows, tok_rows)]
+
+    def tok_copy(k, n, device):
+        return remote(
+            tok_piece(tok, n),
+            tok_piece(toks.at[pos.t], n),
+            tok_send.at[k, n],
+            tok_recv.at[pos.t, n],
+            device,
+        )
+
+    def tok_mate(act):
+        for n in range(TOK_PIECES):
+            act(tok_copy(0, n, pos.at(line=pos.mate, core=pos.low)))
 
     def tok_sends(act):
-        act(tok_copy(0, pos.at(line=pos.mate, core=pos.low)))
-        for k in range(1, cols):
-            act(tok_copy(k, pos.at(col=lax.rem(pos.col + k, cols), core=pos.low)))
-
-        @pl.when(away)
-        def _():
-            act(tok_copy(cols, pos.sibling()))
-
-    def tok_relay(k, c, act):
+        for n in range(TOK_PIECES):
+            for k in range(1, cols):
+                act(tok_copy(k, n, pos.at(col=lax.rem(pos.col + k, cols), core=pos.low)))
+
+            @pl.when(away)
+            def _(n=n):
+                act(tok_copy(cols, n, pos.sibling()))
+
+    def tok_relay(k, c, n, act):
         f = pos.col * 2 + c
+        piece = tok_piece(toks.at[f], n)
         act(
             remote(
-                toks.at[f],
-                toks.at[f],
-                tok_pass.at[k, c],
-                tok_recv.at[f],
+                piece,
+                piece,
+                tok_pass.at[k, c, n],
+                tok_recv.at[f, n],
                 pos.at(col=lax.rem(pos.col + k, cols)),
             )
         )
 
-    def tok_wait(f):
-        remote(toks.at[f], toks.at[f], tok_send.at[0], tok_recv.at[f], pos.sibling()).wait_recv()
+    def tok_wait(f, n):
+        piece = tok_piece(toks.at[f], n)
+        remote(piece, piece, tok_send.at[0, n], tok_recv.at[f, n], pos.sibling()).wait_recv()
 
     params = ((mix_in, mix), (rec_in, rec), (ing_in, ing))
     smalls = ((taps_in, taps), (rate_in, rate), (start_in, start))
@@ -476,28 +539,32 @@
             for k, (src, dst) in enumerate(params)
         ]
 
-    tok_sends(begin)
+    barrier = pltpu.get_barrier_semaphore()
+
+    def greet(device):
+        pl.semaphore_signal(
+            barrier, inc=1, device_id=device, device_id_type=pl.DeviceIdType.MESH
+        )
+
+    for k in range(1, sp):
+        greet(pos.of_run(lax.rem(run + k, sp)))
+    for k in range(1, cols):
+        for c in range(2):
+            greet(pos.at(col=lax.rem(pos.col + k, cols), core=c))
+    for step in (-1, 1):
+
+        @pl.when((line + step >= 0) & (line + step < lines))
+        def _(step=step):
+            for c in range(2):
+                greet(pos.at(line=line + step, core=c))
 
     @pl.when(home)
     def _():
         tok_local().start()
-
-    weights_in.source(begin)
-    weights_in.loaded()
-    weights_in.share(begin)
-    weights_in.first()
-    param_sends(begin)
-
-    @pl.when(home)
-    def _():
         for copy in param_locals():
             copy.start()
         for src, dst in smalls + ((logd_in, logd),):
             dst[...] = src[...]
-
-    weights_out.loaded()
-    weights_out.share(begin)
-    weights_out.first(line=False)
 
     for g in range(tp):
 
@@ -530,32 +597,75 @@
 
     acc[...] = jnp.zeros_like(acc)
 
-    @pl.when(away)
-    def _():
-        for c in range(2):
-            tok_wait(pos.col * 2 + c)
-            for k in range(1, cols):
-                tok_relay(k, c, begin)
+    pl.semaphore_wait(barrier, sp - 1 + 2 * (cols - 1) + jnp.where(pos.outer, 2, 4))
+
+    weights_in.staging(begin)
+    tok_sends(begin)
+    weights_in.loaded()
+    weights_in.share(begin)
+    weights_in.source(begin, wait=True)
+    tok_mate(begin)
+    weights_in.first()
+    param_sends(begin)
+    weights_out.staging(begin)
+    weights_out.loaded()
+    weights_out.share(begin)
+    weights_out.first(line=False)
+
+    def source_out():
+        weights_out.source(begin, wait=True)
+
+    def tok_pass_on(pieces):
+        @pl.when(away)
+        def _():
+            for n in pieces:
+                for c in range(2):
+                    tok_wait(pos.col * 2 + c, n)
+                    for k in range(1, cols):
+                        tok_relay(k, c, n, begin)
+
+
+    @pl.when(pos.outer)
+    def _():
+        source_out()
+        weights_out.first(side=False, wait=False)
 
     weights_in.relay(1)
-    weights_in.crossed(0)
-
-    @pl.loop(2, lines)
+
+    @pl.when(jnp.logical_not(pos.outer))
+    def _():
+        tok_pass_on(range(TOK_PIECES))
+        source_out()
+
+    weights_in.relay(2)
+
+    @pl.when(pos.outer)
+    def _():
+        tok_pass_on(range(TOK_PIECES // 2))
+
+
+    @pl.loop(3, lines)
     def _(d):
         weights_in.relay(d)
-        weights_in.crossed(d - 1)
-
-    weights_out.source(begin)
-    weights_out.first(side=False, wait=False)
+
+
+    @pl.when(pos.outer)
+    def _():
+        tok_pass_on(range(TOK_PIECES // 2, TOK_PIECES))
+
+    weights_in.crossed(0)
+    weights_in.crossed(1)
 
     @pl.when(home)
     def _():
         tok_local().wait()
-        tok_wait(pos.col * 2 + 1 - core)
+        for n in range(TOK_PIECES):
+            tok_wait(pos.col * 2 + 1 - core, n)
 
     for k in range(1, cols):
         for c in range(2):
-            tok_wait(lax.rem(pos.col + k, cols) * 2 + c)
+            for n in range(TOK_PIECES):
+                tok_wait(lax.rem(pos.col + k, cols) * 2 + c, n)
     square = jnp.zeros((count, 1), f32)
     for p in range(tp):
         v = toks[p].astype(f32)
@@ -573,13 +683,15 @@
         for j in range(2):
             acc[j] += jnp.dot(normed[block], win[block, j], preferred_element_type=f32)
 
-    @pl.loop(0, lines - 1)
+    weights_in.use(0, use_in)
+    weights_in.use(1, use_in)
+    @pl.loop(2, lines - 1)
     def _(d):
+        weights_in.crossed(d)
         weights_in.use(d, use_in)
 
     weights_in.crossed(lines - 1)
     weights_in.use(lines - 1, use_in)
-
     ext[halo : halo + count] = acc[0].astype(jnp.bfloat16)
     ulru[...] = acc[1].astype(jnp.bfloat16)
 
@@ -622,6 +734,11 @@
                     act(halo_copy(k, g))
 
     edges(begin)
+
+    @pl.when(jnp.logical_not(pos.outer))
+    def _():
+        weights_out.first(side=False, wait=False)
+
     halos(begin)
 
     @pl.when(home)
@@ -636,18 +753,32 @@
                 dst, dst, par_sem.at[0, k], par_sem.at[1, k], pos.sibling()
             ).wait_recv()
 
-    weights_out.relay(1)
-    weights_out.crossed(0)
+    small = group < tp - 1
+    large = jnp.logical_not(small)
+    weights_out.relay(1, side=False)
+
+    @pl.when(small)
+    def _():
+        weights_out.relay(1, range(PIECES // 2), line=False)
+
     edges(lambda copy: copy.wait_recv(), flip=True)
     wide[0:EDGE] = edge[0].astype(f32)
     wide[EDGE : EDGE + count] = ulru[...].astype(f32)
     wide[EDGE + count :] = edge[1].astype(f32)
     pad = jnp.zeros((8 - logd.shape[0], count), f32)
     decay = jnp.transpose(jnp.concatenate([logd[...], pad], axis=0))
-    gate_stage(wide, taps, rec, ing, rate, decay, keep, drive, count)
-    if lines > 2:
-        weights_out.relay(2)
-        weights_out.crossed(1)
+    heads = rec.shape[1]
+
+    def gates(some):
+        gate_stage(wide, taps, rec, ing, rate, decay, keep, drive, count, some)
+
+    gates(range(heads // 2))
+
+    @pl.when(small)
+    def _():
+        weights_out.relay(1, range(PIECES // 2, PIECES), line=False)
+
+    gates(range(heads // 2, heads))
     ends = scan_stage(keep, drive, count)
     mine[0:4] = run_summary(*ends)
     mine[4:8] = jnp.zeros((4, mine.shape[1]), f32)
@@ -660,9 +791,21 @@
 
     for k in range(1, sp):
         sum_copy(k, run, lax.rem(run + k, sp)).start()
+
+    @pl.when(large)
+    def _():
+        weights_out.relay(1, line=False)
+
+    weights_out.relay(2)
+    weights_out.crossed(0)
     halos(lambda copy: copy.wait_recv(), flip=True)
     grid_rows = count // GRID_W
     y_pool[...] = pool_stage(ext, mix, group, run * grid_rows, sp * grid_rows, count)
+
+    @pl.loop(3, lines)
+    def _(d):
+        weights_out.relay(d)
+
     for k in range(1, sp):
         source = lax.rem(run - k + sp, sp)
         sum_copy(k, source, source).wait_recv()
@@ -686,100 +829,154 @@
             pos.at(col=col),
         )
 
-    def last_copy(c, block, device):
+    def last_copy(row, c, block, device):
         return remote(
-            half_sum.at[block, pl.ds(c * share, share)],
+            part.at[block, pl.ds(pl.multiple_of(row * share, share), share)],
             last.at[1, block],
             last_sem.at[c, block],
             last_sem.at[2, block],
             device,
         )
 
-    def last_near(block):
-        rows = pl.ds(pl.multiple_of((1 - core) * share, share), share)
+    def last_near(row, block):
         return remote(
-            half_sum.at[block, rows],
+            part.at[block, pl.ds(pl.multiple_of(row * share, share), share)],
             last.at[0, block],
-            last_sem.at[0, block],
+            last_sem.at[4, block],
             last_sem.at[3, block],
             pos.sibling(),
         )
 
-    def last_sends(block, act):
-        @pl.when(home)
-        def _():
-            act(last_near(block))
-
-        @pl.when(away)
-        def _():
-            for c in range(2):
-                act(last_copy(c, block, pos.at(line=pos.mate, core=c)))
-
-    def use_out(block):
+    def mate_copy(block):
+        return remote(
+            part.at[block],
+            joined.at[block],
+            mate_sem.at[0, block],
+            mate_sem.at[1, block],
+            pos.at(line=pos.mate),
+        )
+
+    def product(block):
         part[block] = (
             jnp.dot(y_pool[...], wout[block, 0], preferred_element_type=f32)
             + jnp.dot(y_lru[...], wout[block, 1], preferred_element_type=f32)
         ).astype(jnp.bfloat16)
+
+    def keep_mine(row, block):
+        last[0, block] = part[block, pl.ds(pl.multiple_of(row * share, share), share), :]
+
+    def near_sends(block, act):
         for k in range(1, cols):
-            cross_copy(k, block).start()
-
-    def add_half(block):
+            act(cross_copy(k, block))
+
+    def near_last(block, act):
+        @pl.when(home)
+        def _():
+            act(last_near(pos.col * 2 + 1 - core, block))
+
+        @pl.when(away)
+        def _():
+            for c in range(2):
+                act(last_copy(pos.col * 2 + c, c, block, pos.at(line=pos.mate, core=c)))
+
+    def near_out(block):
+        product(block)
+        near_sends(block, begin)
+
+    def near_add(block):
         rows = pl.ds(pl.multiple_of(pos.col * pair, pair), pair)
         total = part[block, rows, :].astype(f32)
         for k in range(1, cols):
             cross_copy(k, block).wait_recv()
             total = total + cross[k - 1, block].astype(f32)
-        half_sum[block] = total.astype(jnp.bfloat16)
-        last_sends(block, begin)
+        part[block, rows, :] = total.astype(jnp.bfloat16)
+        near_last(block, begin)
 
         @pl.when(home)
         def _():
-            mine_rows = pl.ds(pl.multiple_of(core * share, share), share)
-            last[0, block] = half_sum[block, mine_rows, :]
-
-    def collect(d):
-        def both(at):
-            add_half(at * 2 + pos.side)
-            add_half(at * 2 + 1 - pos.side)
-
-        weights_out.around(d, both)
-
-    weights_out.use(0, use_out)
-
-    @pl.loop(min(3, lines), lines)
+            keep_mine(pos.col * 2 + core, block)
+
+    def far_last(block, act):
+        act(last_near(pos.col * 2 + 1 - core, block))
+        for k in range(1, cols):
+            col = lax.rem(pos.col + k, cols)
+            for c in range(2):
+                act(last_copy(col * 2 + c, c, block, pos.at(col=col, core=c)))
+
+    def far_out(block):
+        product(block)
+
+        @pl.when(away)
+        def _():
+            mate_copy(block).start()
+
+    def far_add(block):
+        @pl.when(home)
+        def _():
+            mate_copy(block).wait_recv()
+            part[block] = (
+                part[block].astype(f32) + joined[block].astype(f32)
+            ).astype(jnp.bfloat16)
+            far_last(block, begin)
+            keep_mine(pos.col * 2 + core, block)
+
+    def near_step(d):
+        weights_out.use(d, near_out, (0,))
+
+    def far_step(d):
+        weights_out.use(d, far_out, (1,))
+
+    def near_collect(d):
+        weights_out.around(d, lambda at: near_add(at * 2 + pos.side))
+
+    def far_collect(d):
+        weights_out.around(d, lambda at: far_add(at * 2 + 1 - pos.side))
+
+    near_step(0)
+    near_step(1)
+    near_collect(0)
+
+    @pl.loop(2, lines)
     def _(d):
-        weights_out.relay(d)
+        near_step(d)
+        near_collect(d - 1)
         weights_out.crossed(d - 1)
 
-    @pl.loop(1, lines - 1)
+    far_step(0)
+    near_collect(lines - 1)
+    far_step(1)
+    far_collect(0)
+
+    @pl.loop(2, lines - 1)
     def _(d):
-        weights_out.use(d, use_out)
-        collect(d - 1)
+        far_step(d)
+        far_collect(d - 1)
 
     weights_out.crossed(lines - 1)
-    weights_out.use(lines - 1, use_out)
-    collect(lines - 2)
-    collect(lines - 1)
-
+    far_step(lines - 1)
+    far_collect(lines - 2)
+    far_collect(lines - 1)
     for block in range(sp):
 
         @pl.when(away)
         def _(block=block):
-            last_near(block).wait_recv()
-
-        last_copy(0, block, pos.sibling()).wait_recv()
+            last_near(0, block).wait_recv()
+
+        last_copy(0, 0, block, pos.sibling()).wait_recv()
         total = last[0, block].astype(f32) + last[1, block].astype(f32)
         out[:, block * wide_out : (block + 1) * wide_out] = total.astype(out.dtype)
 
     done = lambda copy: copy.wait_send()
+    tok_mate(done)
     tok_sends(done)
     param_sends(done)
 
     @pl.when(away)
     def _():
-        for c in range(2):
-            for k in range(1, cols):
-                tok_relay(k, c, done)
+        for n in range(TOK_PIECES):
+            for c in range(2):
+                for k in range(1, cols):
+                    tok_relay(k, c, n, done)
 
     weights_in.finish()
     weights_out.finish()
@@ -788,11 +985,20 @@
     for k in range(1, sp):
         sum_copy(k, run, lax.rem(run + k, sp)).wait_send()
 
-    @pl.loop(0, sp)
-    def _(block):
-        for k in range(1, cols):
-            cross_copy(k, block).wait_send()
-        last_sends(block, done)
+    @pl.loop(0, lines)
+    def _(at):
+        block = at * 2 + pos.side
+        near_sends(block, done)
+        near_last(block, done)
+        block = at * 2 + 1 - pos.side
+
+        @pl.when(home)
+        def _():
+            far_last(block, done)
+
+        @pl.when(away)
+        def _():
+            mate_copy(block).wait_send()
 
 
 def per_device(sp, tp, *args):
@@ -809,7 +1015,8 @@
     dma = pltpu.SemaphoreType.DMA
     spread = [
         dma((2,)),
-        dma((2, 2, PIECES)),
+        dma((2, PIECES)),
+        dma((2, PIECES)),
         dma((2, PIECES)),
         dma((3, lines, PIECES)),
         dma((sp, PIECES)),
@@ -838,7 +1045,7 @@
             pltpu.VMEM((count, width), bf16),
             pltpu.VMEM((sp, count, wide_out), bf16),
             pltpu.VMEM((cols - 1, sp, 2 * share, wide_out), bf16),
-            pltpu.VMEM((sp, 2 * share, wide_out), bf16),
+            pltpu.VMEM((sp, count, wide_out), bf16),
             pltpu.VMEM((2, sp, share, wide_out), bf16),
             pltpu.VMEM(pool_mix.shape, bf16),
             pltpu.VMEM(conv_taps.shape, bf16),
@@ -847,11 +1054,13 @@
             pltpu.VMEM(decay_rate.shape, f32),
             pltpu.VMEM(log_decay.shape, f32),
             pltpu.VMEM(start_state.shape, f32),
+            pltpu.VMEM((depth, width), bf16),
+            pltpu.VMEM((width, wide_out), bf16),
             dma((2, 7)),
             dma((1,)),
-            dma((cols + 1,)),
-            dma((cols, 2)),
-            dma((tp,)),
+            dma((cols + 1, TOK_PIECES)),
+            dma((cols, 2, TOK_PIECES)),
+            dma((tp, TOK_PIECES)),
         ]
         + spread
         + spread
@@ -859,10 +1068,11 @@
             dma((2, 4)),
             dma((2, sp)),
             dma((2, cols - 1, sp)),
-            dma((4, sp)),
+            dma((5, sp)),
+            dma((2, sp)),
         ],
         compiler_params=pltpu.CompilerParams(
-            has_side_effects=True, vmem_limit_bytes=60 * 2**20
+            collective_id=0, has_side_effects=True, vmem_limit_bytes=60 * 2**20
         ),
     )(
         tokens,

time: 108 us -> 94.4 us (0.87)
  the two profiles are of different devices: /device:TPU:3 before, /device:TPU:17 now
where the time goes in v2:
time: 94.4 us; the launch traced here: 94.2 us
  Pallas kernels  92.4 us (98%)
  local copies, waits for them, and re-layouts  1.77 us (2%)
    pallas_call x1, Pallas kernels, per_device(): pl.pallas_call(functools.partial(layer_kernel, sp=sp, tp=tp), out_shape=j...  92.4 us

profile of v2, /device:TPU:17, one launch (start us, length us, event | category | flops | bytes accessed | tf_op | source)
XLA Modules:
  0.0 94.2 jit_solution(6255196887349893931)
XLA Ops:
  0.0 92.4 %shard_map.127 = bf16[96,2048]{1,0:T(8,128)(2,1)} custom-call(bf16[384,512]{1,0:T(8,128)(2,1)} %tok.1, f32[1,2048]{1,0:T(1,128)} %bitcast.1, bf16[256,512]{1,0:T(8,128)(2,1)} %wpi.1, bf16[256,512]{1,0:T(8,128)(2,1)} %wli.1, bf16[1,512,512]{2,1,0:T(8,128)(2,1)} %mix_in.1, bf16[4,512]{1,0:T(4,128)(2,1)} %taps_in.1, bf16[2,4,128,128]{3,2,1,0:T(8,128)(2,1)} %rec_in.1, ...), custom_call_target="tpu_custom_call" | custom-call | tf_op jit(solution)/shard_map/pallas_call | solution.py:1025
  92.4 1.8 %copy.15 = bf16[96,2048]{1,0:T(8,128)(2,1)} copy(bf16[96,2048]{1,0:T(8,128)(2,1)} %shard_map.127) | data formatting | bytes 786432

commit v3 on v2

--- a/solution.py
+++ b/solution.py
@@ -15,6 +15,9 @@
 CHUNKS = 8
 PIECES = 4
 TOK_PIECES = 4
+LRU, POOL = (0, 1), (2, 3)
+ALL = LRU + POOL
+HALO_PARTS = 3
 
 
 def one_minus_exp(y):
@@ -174,9 +177,20 @@
         self.src_sem, self.sib_sem, self.line_sem = src_sem, sib_sem, line_sem
         self.pass_sem, self.recv = pass_sem, recv
         self.rows = buf.shape[2] // PIECES
-
-    def piece(self, o, j, p):
-        return self.buf.at[o, j, pl.ds(p * self.rows, self.rows)]
+        self.half = buf.shape[2] // 2
+
+    def rows_of(self, h, p):
+        at = h * self.half + (p % 2) * self.rows
+        return pl.ds(pl.multiple_of(at, self.rows), self.rows)
+
+    def piece(self, o, h, p):
+        return self.buf.at[o, 1 - p // 2, self.rows_of(h, p)]
+
+    def origin(self, h, p):
+        return self.srcs[1 - p // 2].at[self.rows_of(h, p)]
+
+    def staged(self, p):
+        return self.stage.at[pl.ds(p * self.rows, self.rows)]
 
     def load_copy(self, j):
         return pltpu.make_async_copy(self.srcs[j], self.buf.at[self.pos.me, j], self.own.at[j])
@@ -193,56 +207,53 @@
             for j in range(2):
                 self.load_copy(j).wait()
 
-    def rows_of(self, ref, p):
-        return ref.at[pl.ds(p * self.rows, self.rows)]
-
-    def stage_copy(self, j, p):
+    def stage_copy(self, p):
+        pos = self.pos
         return remote(
-            self.rows_of(self.srcs[j], p),
-            self.rows_of(self.stage, p),
+            self.origin(1 - pos.core, p),
+            self.staged(p),
             self.stage_sem.at[0, p],
             self.stage_sem.at[1, p],
-            self.pos.sibling(),
+            pos.sibling(),
         )
 
     def staging(self, act):
-        pos = self.pos
-        for j in range(2):
-
-            @pl.when(jnp.logical_not(pos.home) & (pos.core != j))
-            def _(j=j):
-                for p in range(PIECES):
-                    act(self.stage_copy(j, p))
+        @pl.when(jnp.logical_not(self.pos.home))
+        def _():
+            for p in ALL:
+                act(self.stage_copy(p))
 
     def source_copy(self, src, p, way):
         pos = self.pos
         return remote(
-            self.rows_of(src, p),
+            src,
             self.piece(pos.me, pos.core, p),
             self.src_sem.at[way, p],
             self.recv.at[pos.me, pos.core, p],
             pos.at(line=pos.line + pos.toward * (1 - 2 * way)),
         )
 
-    def source(self, act, wait=False):
+    def source(self, act, pieces=ALL, wait=False):
         pos = self.pos
-        for p in range(PIECES):
-            if wait:
-
-                @pl.when(pos.home)
-                def _(p=p):
-                    self.stage_copy(0, p).wait_recv()
-
-            for way, there in ((0, True), (1, jnp.logical_not(pos.outer))):
-                for src, mine in (
-                    (self.stage, pos.home),
-                    (self.srcs[0], jnp.logical_not(pos.home) & (pos.core == 0)),
-                    (self.srcs[1], jnp.logical_not(pos.home) & (pos.core == 1)),
-                ):
-
-                    @pl.when(mine & there)
-                    def _(src=src, p=p, way=way):
-                        act(self.source_copy(src, p, way))
+
+        def ways(src, p):
+            act(self.source_copy(src, p, 0))
+
+            @pl.when(jnp.logical_not(pos.outer))
+            def _():
+                act(self.source_copy(src, p, 1))
+
+        for p in pieces:
+
+            @pl.when(pos.home)
+            def _(p=p):
+                if wait:
+                    self.stage_copy(p).wait_recv()
+                ways(self.staged(p), p)
+
+            @pl.when(jnp.logical_not(pos.home))
+            def _(p=p):
+                ways(self.origin(pos.core, p), p)
 
     def share_copy(self, j, p):
         pos = self.pos
@@ -254,7 +265,7 @@
     def share(self, act):
         @pl.when(self.pos.home)
         def _():
-            for p in range(PIECES):
+            for p in ALL:
                 for j in (1 - self.pos.core, self.pos.core):
                     act(self.share_copy(j, p))
 
@@ -310,9 +321,9 @@
             def _(line=line):
                 act(line)
 
-    def first(self, line=True, side=True, wait=True):
+    def first(self, pieces=ALL, line=True, side=True, wait=True):
         pos = self.pos
-        for p in range(PIECES):
+        for p in pieces:
             if wait:
 
                 @pl.when(jnp.logical_not(pos.home))
@@ -324,7 +335,7 @@
             if line:
                 self.to_line(pos.line, p, lambda copy: copy.start())
 
-    def relay(self, d, pieces=range(PIECES), line=True, side=True):
+    def relay(self, d, pieces=ALL, line=True, side=True):
         for p in pieces:
 
             def act(at, p=p):
@@ -339,16 +350,16 @@
 
             self.around(d, act)
 
-    def crossed(self, d):
+    def crossed(self, d, pieces=ALL):
         def act(line):
             o = line * 2 + 1 - self.pos.side
-            for p in range(PIECES):
+            for p in pieces:
                 self.await_piece(o, self.pos.core, p)
                 self.to_sibling(o, p, lambda copy: copy.start())
 
         self.around(d, act)
 
-    def use(self, d, act, others=(0, 1)):
+    def use(self, d, act, others=(0, 1), pieces=ALL):
         pos = self.pos
 
         def both(line):
@@ -357,7 +368,7 @@
 
                 @pl.when(jnp.logical_not((o == pos.me) & pos.home))
                 def _():
-                    for p in range(PIECES):
+                    for p in pieces:
                         self.await_piece(o, 1 - pos.core, p)
 
                 act(o)
@@ -603,17 +614,17 @@
     tok_sends(begin)
     weights_in.loaded()
     weights_in.share(begin)
-    weights_in.source(begin, wait=True)
+    weights_in.source(begin, LRU, wait=True)
     tok_mate(begin)
-    weights_in.first()
+    weights_in.first(LRU)
     param_sends(begin)
     weights_out.staging(begin)
     weights_out.loaded()
     weights_out.share(begin)
-    weights_out.first(line=False)
-
-    def source_out():
-        weights_out.source(begin, wait=True)
+
+    def pool_starts():
+        weights_in.source(begin, POOL, wait=True)
+        weights_in.first(POOL)
 
     def tok_pass_on(pieces):
         @pl.when(away)
@@ -624,37 +635,38 @@
                     for k in range(1, cols):
                         tok_relay(k, c, n, begin)
 
-
     @pl.when(pos.outer)
     def _():
-        source_out()
-        weights_out.first(side=False, wait=False)
-
-    weights_in.relay(1)
+        pool_starts()
+        weights_out.first(line=False)
+
+    weights_in.relay(1, LRU)
 
     @pl.when(jnp.logical_not(pos.outer))
     def _():
-        tok_pass_on(range(TOK_PIECES))
-        source_out()
-
-    weights_in.relay(2)
-
-    @pl.when(pos.outer)
-    def _():
-        tok_pass_on(range(TOK_PIECES // 2))
-
+        pool_starts()
+
+    weights_in.relay(2, LRU)
+    tok_pass_on(range(TOK_PIECES))
 
     @pl.loop(3, lines)
     def _(d):
-        weights_in.relay(d)
-
+        weights_in.relay(d, LRU)
+
+    weights_in.crossed(0, LRU)
 
     @pl.when(pos.outer)
     def _():
-        tok_pass_on(range(TOK_PIECES // 2, TOK_PIECES))
-
-    weights_in.crossed(0)
-    weights_in.crossed(1)
+        weights_out.source(begin, wait=True)
+        weights_out.first(side=False, wait=False)
+
+    weights_in.relay(1, POOL)
+
+    @pl.when(jnp.logical_not(pos.outer))
+    def _():
+        weights_out.source(begin, wait=True)
+
+    weights_in.crossed(1, LRU)
 
     @pl.when(home)
     def _():
@@ -679,20 +691,26 @@
                 v * scale * gain[:, at : at + depth]
             ).astype(jnp.bfloat16)
 
-    def use_in(block):
-        for j in range(2):
+    def use_in(j):
+        def act(block):
             acc[j] += jnp.dot(normed[block], win[block, j], preferred_element_type=f32)
 
-    weights_in.use(0, use_in)
-    weights_in.use(1, use_in)
-    @pl.loop(2, lines - 1)
+        return act
+
+    weights_in.use(0, use_in(1), pieces=LRU)
+    weights_in.use(1, use_in(1), pieces=LRU)
+    weights_in.relay(2, POOL)
+
+    @pl.when(jnp.logical_not(pos.outer))
+    def _():
+        weights_out.first(line=False)
+
+
+    @pl.loop(2, lines)
     def _(d):
-        weights_in.crossed(d)
-        weights_in.use(d, use_in)
-
-    weights_in.crossed(lines - 1)
-    weights_in.use(lines - 1, use_in)
-    ext[halo : halo + count] = acc[0].astype(jnp.bfloat16)
+        weights_in.crossed(d, LRU)
+        weights_in.use(d, use_in(1), pieces=LRU)
+
     ulru[...] = acc[1].astype(jnp.bfloat16)
 
     def edge_copy(k):
@@ -700,17 +718,25 @@
             src, dst, device = ulru.at[pl.ds(count - EDGE, EDGE)], edge.at[0], pos.of_run(run + 1)
         else:
             src, dst, device = ulru.at[pl.ds(0, EDGE)], edge.at[1], pos.of_run(run - 1)
-        return remote(src, dst, halo_sem.at[0, k], halo_sem.at[1, k], device)
-
-    def halo_copy(k, g):
-        above, below = 2**g * GRID_W, (2**g - 1) * GRID_W
+        return remote(src, dst, halo_sem.at[0, k, 0], halo_sem.at[1, k, 0], device)
+
+    def halo_copy(k, g, n):
+        rows = 2**g - k
+        low, high = rows * n // HALO_PARTS * GRID_W, rows * (n + 1) // HALO_PARTS * GRID_W
+        if low == high:
+            return None
+        size = high - low
         if k == 0:
-            src = ext.at[pl.ds(halo + count - above, above)]
-            dst, device = ext.at[pl.ds(halo - above, above)], pos.of_run(run + 1)
+            at, to, device = halo + count - rows * GRID_W, halo - rows * GRID_W, run + 1
         else:
-            src = ext.at[pl.ds(halo, below)]
-            dst, device = ext.at[pl.ds(halo + count, below)], pos.of_run(run - 1)
-        return remote(src, dst, halo_sem.at[0, 2 + k], halo_sem.at[1, 2 + k], device)
+            at, to, device = halo, halo + count, run - 1
+        return remote(
+            ext.at[pl.ds(at + low, size)],
+            ext.at[pl.ds(to + low, size)],
+            halo_sem.at[0, 2 + k, n],
+            halo_sem.at[1, 2 + k, n],
+            pos.of_run(device),
+        )
 
     def edges(act, flip=False):
         for k, there in enumerate((run < sp - 1, run > 0)):
@@ -721,25 +747,24 @@
             def _(k=k):
                 act(edge_copy(k))
 
-    def halos(act, flip=False):
+    def halos(act, parts, flip=False):
         for g in range(tp):
             for k, there in enumerate((run < sp - 1, run > 0)):
                 if flip:
                     there = (run > 0, run < sp - 1)[k]
-                if k == 1 and g == 0:
-                    continue
 
                 @pl.when(there & (group == g))
                 def _(k=k, g=g):
-                    act(halo_copy(k, g))
+                    for n in parts:
+                        copy = halo_copy(k, g, n)
+                        if copy is not None:
+                            act(copy)
 
     edges(begin)
 
     @pl.when(jnp.logical_not(pos.outer))
     def _():
         weights_out.first(side=False, wait=False)
-
-    halos(begin)
 
     @pl.when(home)
     def _():
@@ -753,14 +778,24 @@
                 dst, dst, par_sem.at[0, k], par_sem.at[1, k], pos.sibling()
             ).wait_recv()
 
-    small = group < tp - 1
-    large = jnp.logical_not(small)
-    weights_out.relay(1, side=False)
-
-    @pl.when(small)
-    def _():
-        weights_out.relay(1, range(PIECES // 2), line=False)
-
+
+    @pl.loop(3, lines)
+    def _(d):
+        weights_in.relay(d, POOL)
+
+    weights_in.crossed(0, POOL)
+    weights_in.crossed(1, POOL)
+
+    @pl.loop(2, lines)
+    def _(d):
+        weights_in.crossed(d, POOL)
+
+    @pl.loop(0, lines)
+    def _(d):
+        weights_in.use(d, use_in(0), pieces=POOL)
+
+    ext[halo : halo + count] = acc[0].astype(jnp.bfloat16)
+    halos(begin, (0,))
     edges(lambda copy: copy.wait_recv(), flip=True)
     wide[0:EDGE] = edge[0].astype(f32)
     wide[EDGE : EDGE + count] = ulru[...].astype(f32)
@@ -773,10 +808,13 @@
         gate_stage(wide, taps, rec, ing, rate, decay, keep, drive, count, some)
 
     gates(range(heads // 2))
+    halos(begin, (1,))
+    small = group < tp // 2
+    weights_out.relay(1, side=False)
 
     @pl.when(small)
     def _():
-        weights_out.relay(1, range(PIECES // 2, PIECES), line=False)
+        weights_out.relay(1, LRU, line=False)
 
     gates(range(heads // 2, heads))
     ends = scan_stage(keep, drive, count)
@@ -791,21 +829,15 @@
 
     for k in range(1, sp):
         sum_copy(k, run, lax.rem(run + k, sp)).start()
-
-    @pl.when(large)
-    def _():
-        weights_out.relay(1, line=False)
-
+    halos(begin, range(2, HALO_PARTS))
+
+    @pl.when(jnp.logical_not(small))
+    def _():
+        weights_out.relay(1, LRU, line=False)
+
+    weights_out.relay(1, POOL, line=False)
     weights_out.relay(2)
     weights_out.crossed(0)
-    halos(lambda copy: copy.wait_recv(), flip=True)
-    grid_rows = count // GRID_W
-    y_pool[...] = pool_stage(ext, mix, group, run * grid_rows, sp * grid_rows, count)
-
-    @pl.loop(3, lines)
-    def _(d):
-        weights_out.relay(d)
-
     for k in range(1, sp):
         source = lax.rem(run - k + sp, sp)
         sum_copy(k, source, source).wait_recv()
@@ -816,6 +848,14 @@
         enter_b = jnp.where(r > run, sums[r, 2:3] * enter_b + sums[r, 3:4], enter_b)
     close_stage(keep, drive, ends, enter_f, enter_b, y_lru, count)
 
+    @pl.loop(3, lines)
+    def _(d):
+        weights_out.relay(d)
+
+    halos(lambda copy: copy.wait_recv(), range(HALO_PARTS), flip=True)
+    grid_rows = count // GRID_W
+    y_pool[...] = pool_stage(ext, mix, group, run * grid_rows, sp * grid_rows, count)
+
     pair = 2 * share
 
     def cross_copy(k, block):
@@ -865,11 +905,11 @@
     def keep_mine(row, block):
         last[0, block] = part[block, pl.ds(pl.multiple_of(row * share, share), share), :]
 
-    def near_sends(block, act):
+    def even_sends(block, act):
         for k in range(1, cols):
             act(cross_copy(k, block))
 
-    def near_last(block, act):
+    def even_last(block, act):
         @pl.when(home)
         def _():
             act(last_near(pos.col * 2 + 1 - core, block))
@@ -879,83 +919,93 @@
             for c in range(2):
                 act(last_copy(pos.col * 2 + c, c, block, pos.at(line=pos.mate, core=c)))
 
-    def near_out(block):
-        product(block)
-        near_sends(block, begin)
-
-    def near_add(block):
+    def even_add(block):
         rows = pl.ds(pl.multiple_of(pos.col * pair, pair), pair)
         total = part[block, rows, :].astype(f32)
         for k in range(1, cols):
             cross_copy(k, block).wait_recv()
             total = total + cross[k - 1, block].astype(f32)
         part[block, rows, :] = total.astype(jnp.bfloat16)
-        near_last(block, begin)
+        even_last(block, begin)
 
         @pl.when(home)
         def _():
             keep_mine(pos.col * 2 + core, block)
 
-    def far_last(block, act):
+    def odd_last(block, act):
         act(last_near(pos.col * 2 + 1 - core, block))
         for k in range(1, cols):
             col = lax.rem(pos.col + k, cols)
             for c in range(2):
                 act(last_copy(col * 2 + c, c, block, pos.at(col=col, core=c)))
 
-    def far_out(block):
-        product(block)
-
-        @pl.when(away)
-        def _():
-            mate_copy(block).start()
-
-    def far_add(block):
+    def odd_add(block):
         @pl.when(home)
         def _():
             mate_copy(block).wait_recv()
             part[block] = (
                 part[block].astype(f32) + joined[block].astype(f32)
             ).astype(jnp.bfloat16)
-            far_last(block, begin)
+            odd_last(block, begin)
             keep_mine(pos.col * 2 + core, block)
 
-    def near_step(d):
-        weights_out.use(d, near_out, (0,))
-
-    def far_step(d):
-        weights_out.use(d, far_out, (1,))
-
-    def near_collect(d):
-        weights_out.around(d, lambda at: near_add(at * 2 + pos.side))
-
-    def far_collect(d):
-        weights_out.around(d, lambda at: far_add(at * 2 + 1 - pos.side))
-
-    near_step(0)
-    near_step(1)
-    near_collect(0)
+    def is_even(block):
+        return lax.rem(block // 2, 2) == 0
+
+    def produce(block):
+        product(block)
+
+        @pl.when(is_even(block))
+        def _():
+            even_sends(block, begin)
+
+        @pl.when(jnp.logical_not(is_even(block)) & away)
+        def _():
+            mate_copy(block).start()
+
+    def gather(block):
+        @pl.when(is_even(block))
+        def _():
+            even_add(block)
+
+        @pl.when(jnp.logical_not(is_even(block)))
+        def _():
+            odd_add(block)
+
+    def step(d, other):
+        weights_out.use(d, produce, (other,))
+
+    def collect(d, other):
+        weights_out.around(
+            d, lambda at: gather(at * 2 + (1 - pos.side if other else pos.side))
+        )
+
+
+    @pl.loop(0, lines)
+    def _(d):
+        step(d, 0)
+
+    step(0, 1)
+    collect(0, 0)
+    collect(1, 0)
+    weights_out.crossed(1)
+    step(1, 1)
 
     @pl.loop(2, lines)
     def _(d):
-        near_step(d)
-        near_collect(d - 1)
-        weights_out.crossed(d - 1)
-
-    far_step(0)
-    near_collect(lines - 1)
-    far_step(1)
-    far_collect(0)
-
-    @pl.loop(2, lines - 1)
+        collect(d, 0)
+
+
+    @pl.loop(2, lines)
     def _(d):
-        far_step(d)
-        far_collect(d - 1)
-
-    weights_out.crossed(lines - 1)
-    far_step(lines - 1)
-    far_collect(lines - 2)
-    far_collect(lines - 1)
+        weights_out.crossed(d)
+        step(d, 1)
+
+
+    @pl.loop(0, lines)
+    def _(d):
+        collect(d, 1)
+
     for block in range(sp):
 
         @pl.when(away)
@@ -981,22 +1031,22 @@
     weights_in.finish()
     weights_out.finish()
     edges(done)
-    halos(done)
+    halos(done, range(HALO_PARTS))
     for k in range(1, sp):
         sum_copy(k, run, lax.rem(run + k, sp)).wait_send()
 
-    @pl.loop(0, lines)
-    def _(at):
-        block = at * 2 + pos.side
-        near_sends(block, done)
-        near_last(block, done)
-        block = at * 2 + 1 - pos.side
-
-        @pl.when(home)
-        def _():
-            far_last(block, done)
-
-        @pl.when(away)
+    @pl.loop(0, sp)
+    def _(block):
+        @pl.when(is_even(block))
+        def _():
+            even_sends(block, done)
+            even_last(block, done)
+
+        @pl.when(jnp.logical_not(is_even(block)) & home)
+        def _():
+            odd_last(block, done)
+
+        @pl.when(jnp.logical_not(is_even(block)) & away)
         def _():
             mate_copy(block).wait_send()
 
@@ -1065,7 +1115,7 @@
         + spread
         + spread
         + [
-            dma((2, 4)),
+            dma((2, 4, HALO_PARTS)),
             dma((2, sp)),
             dma((2, cols - 1, sp)),
             dma((5, sp)),

time: 94.4 us -> 89.7 us (0.950)
  the two profiles are of different devices: /device:TPU:17 before, /device:TPU:3 now
where the time goes in v3:
time: 89.7 us; the launch traced here: 88.7 us
  Pallas kernels  86.9 us (97%)
  local copies, waits for them, and re-layouts  1.77 us (2%)
    pallas_call x1, Pallas kernels, per_device(): pl.pallas_call(functools.partial(layer_kernel, sp=sp, tp=tp), out_shape=j...  86.9 us

profile of v3, /device:TPU:3, one launch (start us, length us, event | category | flops | bytes accessed | tf_op | source)
XLA Modules:
  0.0 88.7 jit_solution(8712456736859298587)
XLA Ops:
  0.0 86.9 %shard_map.127 = bf16[96,2048]{1,0:T(8,128)(2,1)} custom-call(bf16[384,512]{1,0:T(8,128)(2,1)} %tok.1, f32[1,2048]{1,0:T(1,128)} %bitcast.1, bf16[256,512]{1,0:T(8,128)(2,1)} %wpi.1, bf16[256,512]{1,0:T(8,128)(2,1)} %wli.1, bf16[1,512,512]{2,1,0:T(8,128)(2,1)} %mix_in.1, bf16[4,512]{1,0:T(4,128)(2,1)} %taps_in.1, bf16[2,4,128,128]{3,2,1,0:T(8,128)(2,1)} %rec_in.1, ...), custom_call_target="tpu_custom_call" | custom-call | tf_op jit(solution)/shard_map/pallas_call | solution.py:1075
  86.9 1.8 %copy.15 = bf16[96,2048]{1,0:T(8,128)(2,1)} copy(bf16[96,2048]{1,0:T(8,128)(2,1)} %shard_map.127) | data formatting | bytes 786432

commit v4 on v3

--- a/solution.py
+++ b/solution.py
@@ -171,7 +171,8 @@
 
 
 class Spread:
-    def __init__(self, place, srcs, buf, stage, own, stage_sem, src_sem, sib_sem, line_sem, pass_sem, recv):
+    def __init__(self, place, srcs, buf, stage, own, stage_sem, src_sem, sib_sem, line_sem, pass_sem, recv, swaps=None):
+        self.swaps = swaps
         self.pos, self.srcs, self.buf, self.own = place, srcs, buf, own
         self.stage, self.stage_sem = stage, stage_sem
         self.src_sem, self.sib_sem, self.line_sem = src_sem, sib_sem, line_sem
@@ -183,11 +184,22 @@
         at = h * self.half + (p % 2) * self.rows
         return pl.ds(pl.multiple_of(at, self.rows), self.rows)
 
-    def piece(self, o, h, p):
-        return self.buf.at[o, 1 - p // 2, self.rows_of(h, p)]
-
-    def origin(self, h, p):
-        return self.srcs[1 - p // 2].at[self.rows_of(h, p)]
+    def matrix(self, p, which=0):
+        first = 1 - p // 2
+        return first if self.swaps is None else jnp.where(self.swaps[which], 1 - first, first)
+
+    def piece(self, o, h, p, which=0):
+        return self.buf.at[o, self.matrix(p, which), self.rows_of(h, p)]
+
+    def from_origin(self, h, p, act):
+        if self.swaps is None:
+            act(self.srcs[1 - p // 2].at[self.rows_of(h, p)])
+            return
+        for flag, j in ((jnp.logical_not(self.swaps[1]), 1 - p // 2), (self.swaps[1], p // 2)):
+
+            @pl.when(flag)
+            def _(j=j):
+                act(self.srcs[j].at[self.rows_of(h, p)])
 
     def staged(self, p):
         return self.stage.at[pl.ds(p * self.rows, self.rows)]
@@ -207,28 +219,29 @@
             for j in range(2):
                 self.load_copy(j).wait()
 
-    def stage_copy(self, p):
+    def stage_copy(self, p, src):
+        return remote(
+            src,
+            self.staged(p),
+            self.stage_sem.at[PIECES],
+            self.stage_sem.at[p],
+            self.pos.sibling(),
+        )
+
+    def staging(self, act):
         pos = self.pos
-        return remote(
-            self.origin(1 - pos.core, p),
-            self.staged(p),
-            self.stage_sem.at[0, p],
-            self.stage_sem.at[1, p],
-            pos.sibling(),
-        )
-
-    def staging(self, act):
-        @pl.when(jnp.logical_not(self.pos.home))
+
+        @pl.when(jnp.logical_not(pos.home))
         def _():
             for p in ALL:
-                act(self.stage_copy(p))
+                self.from_origin(1 - pos.core, p, lambda src, p=p: act(self.stage_copy(p, src)))
 
     def source_copy(self, src, p, way):
         pos = self.pos
         return remote(
             src,
-            self.piece(pos.me, pos.core, p),
-            self.src_sem.at[way, p],
+            self.piece(pos.me, pos.core, p, 1),
+            self.src_sem.at[way],
             self.recv.at[pos.me, pos.core, p],
             pos.at(line=pos.line + pos.toward * (1 - 2 * way)),
         )
@@ -248,19 +261,17 @@
             @pl.when(pos.home)
             def _(p=p):
                 if wait:
-                    self.stage_copy(p).wait_recv()
+                    self.stage_copy(p, self.staged(p)).wait_recv()
                 ways(self.staged(p), p)
 
             @pl.when(jnp.logical_not(pos.home))
             def _(p=p):
-                ways(self.origin(pos.core, p), p)
+                self.from_origin(pos.core, p, lambda src: ways(src, p))
 
     def share_copy(self, j, p):
         pos = self.pos
         piece = self.piece(pos.me, j, p)
-        return remote(
-            piece, piece, self.sib_sem.at[j, p], self.recv.at[pos.me, j, p], pos.sibling()
-        )
+        return remote(piece, piece, self.sib_sem.at[0], self.recv.at[pos.me, j, p], pos.sibling())
 
     def share(self, act):
         @pl.when(self.pos.home)
@@ -269,13 +280,14 @@
                 for j in (1 - self.pos.core, self.pos.core):
                     act(self.share_copy(j, p))
 
+    def carried(self, o, p):
+        return self.buf.at[o, 0] if p is None else self.piece(o, self.pos.core, p)
+
     def block(self, line, p, kind, device):
-        pos = self.pos
-        o = line * 2 + pos.side
-        piece = self.piece(o, pos.core, p)
-        return remote(
-            piece, piece, self.line_sem.at[kind, line, p], self.recv.at[o, pos.core, p], device
-        )
+        o = line * 2 + self.pos.side
+        piece = self.carried(o, p)
+        recv = self.recv.at[o, self.pos.core, 0 if p is None else p]
+        return remote(piece, piece, self.line_sem.at[kind, line], recv, device)
 
     def to_line(self, line, p, act):
         pos = self.pos
@@ -292,21 +304,14 @@
         act(self.block(line, p, 2, self.pos.at(side=1 - self.pos.side)))
 
     def to_sibling(self, o, p, act):
-        piece = self.piece(o, self.pos.core, p)
-        act(
-            remote(
-                piece,
-                piece,
-                self.pass_sem.at[o, p],
-                self.recv.at[o, self.pos.core, p],
-                self.pos.sibling(),
-            )
-        )
+        piece = self.carried(o, p)
+        recv = self.recv.at[o, self.pos.core, 0 if p is None else p]
+        act(remote(piece, piece, self.pass_sem.at[o], recv, self.pos.sibling()))
 
     def await_piece(self, o, j, p):
         piece = self.piece(o, j, p)
         remote(
-            piece, piece, self.pass_sem.at[o, p], self.recv.at[o, j, p], self.pos.sibling()
+            piece, piece, self.pass_sem.at[o], self.recv.at[o, j, p], self.pos.sibling()
         ).wait_recv()
 
     def around(self, d, act):
@@ -378,21 +383,42 @@
     def finish(self):
         pos = self.pos
         done = lambda copy: copy.wait_send()
-        self.staging(done)
-        self.source(done)
-        self.share(done)
+
+        @pl.when(jnp.logical_not(pos.home))
+        def _():
+            self.stage_copy_all().wait_send()
+
+        for way, there in ((0, True), (1, jnp.logical_not(pos.outer))):
+
+            @pl.when(there)
+            def _(way=way):
+                whole = self.buf.at[pos.me, 0]
+                remote(
+                    whole, whole, self.src_sem.at[way], self.recv.at[pos.me, 0, 0], pos.sibling()
+                ).wait_send()
+
+        @pl.when(pos.home)
+        def _():
+            whole = self.buf.at[pos.me]
+            remote(
+                whole, whole, self.sib_sem.at[0], self.recv.at[pos.me, 0, 0], pos.sibling()
+            ).wait_send()
 
         @pl.loop(0, pos.lines)
         def _(line):
-            for p in range(PIECES):
-                self.to_line(line, p, done)
-                self.to_side(line, p, done)
-
-                @pl.when(line != pos.line)
-                def _():
-                    self.to_sibling(line * 2 + pos.side, p, done)
-
-                self.to_sibling(line * 2 + 1 - pos.side, p, done)
+            self.to_line(line, None, done)
+            self.to_side(line, None, done)
+
+            @pl.when(line != pos.line)
+            def _():
+                self.to_sibling(line * 2 + pos.side, None, done)
+
+            self.to_sibling(line * 2 + 1 - pos.side, None, done)
+
+    def stage_copy_all(self):
+        return remote(
+            self.stage, self.stage, self.stage_sem.at[PIECES], self.stage_sem.at[0], self.pos.sibling()
+        )
 
 
 def layer_kernel(
@@ -477,11 +503,14 @@
     halo = REACH * GRID_W
     lines, cols = pos.lines, pos.cols
 
+    swap = group == tp - 1
+    keep_order = jnp.logical_not(swap)
     weights_in = Spread(
-        pos, (wpi, wli), win, in_stage, in_own, in_stg, in_src, in_sib, in_line, in_pass, in_recv
+        pos, (wpi, wli), win, in_stage, in_own, in_stg, in_src, in_sib, in_line, in_pass, in_recv,
+        swaps=(swap, pos.col * 2 + 1 - pos.low == tp - 1),
     )
     weights_out = Spread(
-        pos, (wpo, wlo), wout, out_stage, out_own, out_stg, out_src, out_sib, out_line, out_pass, out_recv
+        pos, (wpo, wlo), wout, out_stage, out_own, out_stg, out_src, out_sib, out_line, out_pass, out_recv,
     )
     weights_in.load()
     weights_out.load()
@@ -495,20 +524,17 @@
         return ref.at[pl.ds(n * tok_rows, tok_rows)]
 
     def tok_copy(k, n, device):
-        return remote(
-            tok_piece(tok, n),
-            tok_piece(toks.at[pos.t], n),
-            tok_send.at[k, n],
-            tok_recv.at[pos.t, n],
-            device,
-        )
-
-    def tok_mate(act):
-        for n in range(TOK_PIECES):
+        src, dst = tok, toks.at[pos.t]
+        if n is not None:
+            src, dst = tok_piece(src, n), tok_piece(dst, n)
+        return remote(src, dst, tok_send.at[k], tok_recv.at[pos.t, n or 0], device)
+
+    def tok_mate(act, pieces=range(TOK_PIECES)):
+        for n in pieces:
             act(tok_copy(0, n, pos.at(line=pos.mate, core=pos.low)))
 
-    def tok_sends(act):
-        for n in range(TOK_PIECES):
+    def tok_sends(act, pieces=range(TOK_PIECES)):
+        for n in pieces:
             for k in range(1, cols):
                 act(tok_copy(k, n, pos.at(col=lax.rem(pos.col + k, cols), core=pos.low)))
 
@@ -518,20 +544,20 @@
 
     def tok_relay(k, c, n, act):
         f = pos.col * 2 + c
-        piece = tok_piece(toks.at[f], n)
+        piece = toks.at[f] if n is None else tok_piece(toks.at[f], n)
         act(
             remote(
                 piece,
                 piece,
-                tok_pass.at[k, c, n],
-                tok_recv.at[f, n],
+                tok_pass.at[k, c],
+                tok_recv.at[f, n or 0],
                 pos.at(col=lax.rem(pos.col + k, cols)),
             )
         )
 
     def tok_wait(f, n):
         piece = tok_piece(toks.at[f], n)
-        remote(piece, piece, tok_send.at[0, n], tok_recv.at[f, n], pos.sibling()).wait_recv()
+        remote(piece, piece, tok_send.at[0], tok_recv.at[f, n], pos.sibling()).wait_recv()
 
     params = ((mix_in, mix), (rec_in, rec), (ing_in, ing))
     smalls = ((taps_in, taps), (rate_in, rate), (start_in, start))
@@ -610,12 +636,22 @@
 
     pl.semaphore_wait(barrier, sp - 1 + 2 * (cols - 1) + jnp.where(pos.outer, 2, 4))
 
+    inner = jnp.logical_not(pos.outer)
     weights_in.staging(begin)
     tok_sends(begin)
+
+    @pl.when(inner)
+    def _():
+        tok_mate(begin)
+
     weights_in.loaded()
     weights_in.share(begin)
     weights_in.source(begin, LRU, wait=True)
-    tok_mate(begin)
+
+    @pl.when(pos.outer)
+    def _():
+        tok_mate(begin)
+
     weights_in.first(LRU)
     param_sends(begin)
     weights_out.staging(begin)
@@ -639,33 +675,34 @@
     def _():
         pool_starts()
         weights_out.first(line=False)
-
-    weights_in.relay(1, LRU)
-
-    @pl.when(jnp.logical_not(pos.outer))
-    def _():
+        weights_out.source(begin, wait=True)
+        weights_out.first(side=False, wait=False)
+        weights_in.relay(2, LRU)
+        tok_pass_on(range(TOK_PIECES))
+        weights_in.relay(1, LRU)
+
+    @pl.when(inner)
+    def _():
+        weights_in.relay(1, LRU)
         pool_starts()
-
-    weights_in.relay(2, LRU)
-    tok_pass_on(range(TOK_PIECES))
+        tok_pass_on(range(TOK_PIECES))
+        weights_in.relay(2, LRU)
+
 
     @pl.loop(3, lines)
     def _(d):
         weights_in.relay(d, LRU)
 
+
+    @pl.when(pos.outer)
+    def _():
+        weights_in.relay(2, POOL)
+
+    @pl.when(inner)
+    def _():
+        weights_in.relay(1, POOL)
+
     weights_in.crossed(0, LRU)
-
-    @pl.when(pos.outer)
-    def _():
-        weights_out.source(begin, wait=True)
-        weights_out.first(side=False, wait=False)
-
-    weights_in.relay(1, POOL)
-
-    @pl.when(jnp.logical_not(pos.outer))
-    def _():
-        weights_out.source(begin, wait=True)
-
     weights_in.crossed(1, LRU)
 
     @pl.when(home)
@@ -691,38 +728,53 @@
                 v * scale * gain[:, at : at + depth]
             ).astype(jnp.bfloat16)
 
-    def use_in(j):
+    def use_in(p):
+        j = weights_in.matrix(p)
+
         def act(block):
             acc[j] += jnp.dot(normed[block], win[block, j], preferred_element_type=f32)
 
         return act
 
-    weights_in.use(0, use_in(1), pieces=LRU)
-    weights_in.use(1, use_in(1), pieces=LRU)
-    weights_in.relay(2, POOL)
-
-    @pl.when(jnp.logical_not(pos.outer))
+    weights_in.use(0, use_in(LRU[0]), pieces=LRU)
+    weights_in.use(1, use_in(LRU[0]), pieces=LRU)
+
+    @pl.when(pos.outer)
+    def _():
+        weights_in.relay(1, POOL)
+
+    @pl.when(inner)
+    def _():
+        weights_in.relay(2, POOL)
+
+    @pl.when(inner & keep_order)
     def _():
         weights_out.first(line=False)
+
+
+    @pl.loop(3, lines)
+    def _(d):
+        weights_in.relay(d, POOL)
 
 
     @pl.loop(2, lines)
     def _(d):
         weights_in.crossed(d, LRU)
-        weights_in.use(d, use_in(1), pieces=LRU)
-
-    ulru[...] = acc[1].astype(jnp.bfloat16)
+        weights_in.use(d, use_in(LRU[0]), pieces=LRU)
+
 
     def edge_copy(k):
         if k == 0:
             src, dst, device = ulru.at[pl.ds(count - EDGE, EDGE)], edge.at[0], pos.of_run(run + 1)
         else:
             src, dst, device = ulru.at[pl.ds(0, EDGE)], edge.at[1], pos.of_run(run - 1)
-        return remote(src, dst, halo_sem.at[0, k, 0], halo_sem.at[1, k, 0], device)
+        return remote(src, dst, halo_sem.at[0, k], halo_sem.at[1, k], device)
 
     def halo_copy(k, g, n):
         rows = 2**g - k
-        low, high = rows * n // HALO_PARTS * GRID_W, rows * (n + 1) // HALO_PARTS * GRID_W
+        low, high = 0, rows * GRID_W
+        if n is not None:
+            low, high = (rows * m // HALO_PARTS * GRID_W for m in (n, n + 1))
         if low == high:
             return None
         size = high - low
@@ -733,8 +785,8 @@
         return remote(
             ext.at[pl.ds(at + low, size)],
             ext.at[pl.ds(to + low, size)],
-            halo_sem.at[0, 2 + k, n],
-            halo_sem.at[1, 2 + k, n],
+            halo_sem.at[0, 2 + k],
+            halo_sem.at[1, 2 + k],
             pos.of_run(device),
         )
 
@@ -760,11 +812,33 @@
                         if copy is not None:
                             act(copy)
 
-    edges(begin)
-
-    @pl.when(jnp.logical_not(pos.outer))
+    def end_lru():
+        ulru[...] = acc[1].astype(jnp.bfloat16)
+        edges(begin)
+
+    def end_pool(parts):
+        ext[halo : halo + count] = acc[0].astype(jnp.bfloat16)
+        halos(begin, parts)
+
+    @pl.when(keep_order)
+    def _():
+        end_lru()
+
+    @pl.when(swap)
+    def _():
+        end_pool((0,))
+
+    @pl.when(inner)
+    def _():
+        weights_out.source(begin, wait=True)
+
+    @pl.when(inner & keep_order)
     def _():
         weights_out.first(side=False, wait=False)
+
+    @pl.when(inner & swap)
+    def _():
+        weights_out.first(side=False)
 
     @pl.when(home)
     def _():
@@ -779,23 +853,27 @@
             ).wait_recv()
 
 
-    @pl.loop(3, lines)
-    def _(d):
-        weights_in.relay(d, POOL)
-
-    weights_in.crossed(0, POOL)
-    weights_in.crossed(1, POOL)
-
-    @pl.loop(2, lines)
+    @pl.loop(0, lines)
     def _(d):
         weights_in.crossed(d, POOL)
 
     @pl.loop(0, lines)
     def _(d):
-        weights_in.use(d, use_in(0), pieces=POOL)
-
-    ext[halo : halo + count] = acc[0].astype(jnp.bfloat16)
-    halos(begin, (0,))
+        weights_in.use(d, use_in(POOL[0]), pieces=POOL)
+
+    @pl.when(keep_order)
+    def _():
+        end_pool((0,))
+
+    @pl.when(swap)
+    def _():
+        end_lru()
+        halos(begin, range(1, HALO_PARTS))
+
+    @pl.when(inner & swap)
+    def _():
+        weights_out.first(line=False, wait=False)
+
     edges(lambda copy: copy.wait_recv(), flip=True)
     wide[0:EDGE] = edge[0].astype(f32)
     wide[EDGE : EDGE + count] = ulru[...].astype(f32)
@@ -808,13 +886,16 @@
         gate_stage(wide, taps, rec, ing, rate, decay, keep, drive, count, some)
 
     gates(range(heads // 2))
-    halos(begin, (1,))
     small = group < tp // 2
-    weights_out.relay(1, side=False)
+
+    @pl.when(keep_order)
+    def _():
+        halos(begin, (1,))
+
 
     @pl.when(small)
     def _():
-        weights_out.relay(1, LRU, line=False)
+        weights_out.relay(1, LRU)
 
     gates(range(heads // 2, heads))
     ends = scan_stage(keep, drive, count)
@@ -824,35 +905,35 @@
 
     def sum_copy(k, source, target):
         return remote(
-            mine, sums.at[source], sum_sem.at[0, k], sum_sem.at[1, k], pos.of_run(target)
+            mine, sums.at[source], sum_sem.at[0], sum_sem.at[1], pos.of_run(target)
         )
+
+    def sum_all():
+        every = sums.at[pl.ds(0, sp - 1)]
+        return remote(every, every, sum_sem.at[0], sum_sem.at[1], pos.sibling())
 
     for k in range(1, sp):
         sum_copy(k, run, lax.rem(run + k, sp)).start()
-    halos(begin, range(2, HALO_PARTS))
+
+    @pl.when(keep_order)
+    def _():
+        halos(begin, range(2, HALO_PARTS))
 
     @pl.when(jnp.logical_not(small))
     def _():
-        weights_out.relay(1, LRU, line=False)
-
-    weights_out.relay(1, POOL, line=False)
+        weights_out.relay(1, LRU)
+
+    weights_out.relay(1, POOL)
     weights_out.relay(2)
     weights_out.crossed(0)
-    for k in range(1, sp):
-        source = lax.rem(run - k + sp, sp)
-        sum_copy(k, source, source).wait_recv()
+    sum_all().wait_recv()
     enter_f, enter_b = start[0:1], start[1:2]
     for s in range(sp - 1):
         r = sp - 1 - s
         enter_f = jnp.where(s < run, sums[s, 0:1] * enter_f + sums[s, 1:2], enter_f)
         enter_b = jnp.where(r > run, sums[r, 2:3] * enter_b + sums[r, 3:4], enter_b)
     close_stage(keep, drive, ends, enter_f, enter_b, y_lru, count)
-
-    @pl.loop(3, lines)
-    def _(d):
-        weights_out.relay(d)
-
-    halos(lambda copy: copy.wait_recv(), range(HALO_PARTS), flip=True)
+    halos(lambda copy: copy.wait_recv(), (None,), flip=True)
     grid_rows = count // GRID_W
     y_pool[...] = pool_stage(ext, mix, group, run * grid_rows, sp * grid_rows, count)
 
@@ -864,17 +945,17 @@
         return remote(
             part.at[block, rows],
             cross.at[k - 1, block],
-            cross_sem.at[0, k - 1, block],
-            cross_sem.at[1, k - 1, block],
+            cross_sem.at[k - 1, sp],
+            cross_sem.at[k - 1, block],
             pos.at(col=col),
         )
 
-    def last_copy(row, c, block, device):
+    def last_copy(row, k, block, device):
         return remote(
             part.at[block, pl.ds(pl.multiple_of(row * share, share), share)],
             last.at[1, block],
-            last_sem.at[c, block],
-            last_sem.at[2, block],
+            last_sem.at[3 + k],
+            last_sem.at[1],
             device,
         )
 
@@ -882,17 +963,21 @@
         return remote(
             part.at[block, pl.ds(pl.multiple_of(row * share, share), share)],
             last.at[0, block],
-            last_sem.at[4, block],
-            last_sem.at[3, block],
+            last_sem.at[0],
+            last_sem.at[2],
             pos.sibling(),
         )
+
+    def last_all(which, send, recv):
+        every = last.at[which]
+        return remote(every, every, last_sem.at[send], last_sem.at[recv], pos.sibling())
 
     def mate_copy(block):
         return remote(
             part.at[block],
             joined.at[block],
-            mate_sem.at[0, block],
-            mate_sem.at[1, block],
+            mate_sem.at[sp],
+            mate_sem.at[block],
             pos.at(line=pos.mate),
         )
 
@@ -917,7 +1002,7 @@
         @pl.when(away)
         def _():
             for c in range(2):
-                act(last_copy(pos.col * 2 + c, c, block, pos.at(line=pos.mate, core=c)))
+                act(last_copy(pos.col * 2 + c, 0, block, pos.at(line=pos.mate, core=c)))
 
     def even_add(block):
         rows = pl.ds(pl.multiple_of(pos.col * pair, pair), pair)
@@ -937,7 +1022,7 @@
         for k in range(1, cols):
             col = lax.rem(pos.col + k, cols)
             for c in range(2):
-                act(last_copy(col * 2 + c, c, block, pos.at(col=col, core=c)))
+                act(last_copy(col * 2 + c, k - 1, block, pos.at(col=col, core=c)))
 
     def odd_add(block):
         @pl.when(home)
@@ -981,11 +1066,15 @@
         )
 
 
-    @pl.loop(0, lines)
+    for d in range(min(3, lines)):
+        step(d, 0)
+    step(0, 1)
+
+    @pl.loop(3, lines)
     def _(d):
+        weights_out.relay(d)
         step(d, 0)
 
-    step(0, 1)
     collect(0, 0)
     collect(1, 0)
     weights_out.crossed(1)
@@ -1006,49 +1095,51 @@
     def _(d):
         collect(d, 1)
 
+
+    @pl.when(away)
+    def _():
+        last_all(0, 0, 2).wait_recv()
+
+    last_all(1, 0, 1).wait_recv()
     for block in range(sp):
-
-        @pl.when(away)
-        def _(block=block):
-            last_near(0, block).wait_recv()
-
-        last_copy(0, 0, block, pos.sibling()).wait_recv()
         total = last[0, block].astype(f32) + last[1, block].astype(f32)
         out[:, block * wide_out : (block + 1) * wide_out] = total.astype(out.dtype)
 
     done = lambda copy: copy.wait_send()
-    tok_mate(done)
-    tok_sends(done)
+    tok_mate(done, (None,))
+    tok_sends(done, (None,))
     param_sends(done)
 
     @pl.when(away)
     def _():
-        for n in range(TOK_PIECES):
-            for c in range(2):
-                for k in range(1, cols):
-                    tok_relay(k, c, n, done)
+        for c in range(2):
+            for k in range(1, cols):
+                tok_relay(k, c, None, done)
 
     weights_in.finish()
     weights_out.finish()
     edges(done)
-    halos(done, range(HALO_PARTS))
-    for k in range(1, sp):
-        sum_copy(k, run, lax.rem(run + k, sp)).wait_send()
-
-    @pl.loop(0, sp)
-    def _(block):
-        @pl.when(is_even(block))
-        def _():
-            even_sends(block, done)
-            even_last(block, done)
-
-        @pl.when(jnp.logical_not(is_even(block)) & home)
-        def _():
-            odd_last(block, done)
-
-        @pl.when(jnp.logical_not(is_even(block)) & away)
-        def _():
-            mate_copy(block).wait_send()
+    halos(done, (None,))
+    sum_all().wait_send()
+
+    half = pl.ds(0, sp // 2)
+    for k in range(1, cols):
+        every = cross.at[k - 1, half]
+        remote(
+            every, every, cross_sem.at[k - 1, sp], cross_sem.at[k - 1, 0], pos.sibling()
+        ).wait_send()
+
+    @pl.when(home)
+    def _():
+        last_all(0, 0, 2).wait_send()
+        for k in range(1, cols):
+            last_all(1, 2 + k, 1).wait_send()
+
+    @pl.when(away)
+    def _():
+        last_all(1, 3, 1).wait_send()
+        every = part.at[half]
+        remote(every, every, mate_sem.at[sp], mate_sem.at[0], pos.sibling()).wait_send()
 
 
 def per_device(sp, tp, *args):
@@ -1065,11 +1156,11 @@
     dma = pltpu.SemaphoreType.DMA
     spread = [
         dma((2,)),
-        dma((2, PIECES)),
-        dma((2, PIECES)),
-        dma((2, PIECES)),
-        dma((3, lines, PIECES)),
-        dma((sp, PIECES)),
+        dma((PIECES + 1,)),
+        dma((2,)),
+        dma((1,)),
+        dma((3, lines)),
+        dma((sp,)),
         dma((sp, 2, PIECES)),
     ]
     return pl.pallas_call(
@@ -1108,18 +1199,18 @@
             pltpu.VMEM((width, wide_out), bf16),
             dma((2, 7)),
             dma((1,)),
-            dma((cols + 1, TOK_PIECES)),
-            dma((cols, 2, TOK_PIECES)),
+            dma((cols + 1,)),
+            dma((cols, 2)),
             dma((tp, TOK_PIECES)),
         ]
         + spread
         + spread
         + [
-            dma((2, 4, HALO_PARTS)),
-            dma((2, sp)),
-            dma((2, cols - 1, sp)),
-            dma((5, sp)),
-            dma((2, sp)),
+            dma((2, 4)),
+            dma((2,)),
+            dma((cols - 1, sp + 1)),
+            dma((2 + cols,)),
+            dma((sp + 1,)),
         ],
         compiler_params=pltpu.CompilerParams(
             collective_id=0, has_side_effects=True, vmem_limit_bytes=60 * 2**20

time: 89.7 us -> 85.4 us (0.952)
  Pallas kernels: 86.9 us -> 82.4 us
    pallas_call x1, Pallas kernels: 86.9 us -> 82.4 us  [per_device(): pl.pallas_call(functools.partial(layer_kernel, sp=sp, tp=tp), out_shape=j...]
where the time goes in v4:
time: 85.4 us; the launch traced here: 84.2 us
  Pallas kernels  82.4 us (96%)
  local copies, waits for them, and re-layouts  1.77 us (2%)
    pallas_call x1, Pallas kernels, per_device(): pl.pallas_call(functools.partial(layer_kernel, sp=sp, tp=tp), out_shape=j...  82.4 us
    unnamed x1, local copies, waits for them, and re-layouts  1.77 us

profile of v4, /device:TPU:3, one launch (start us, length us, event | category | flops | bytes accessed | tf_op | source)
XLA Modules:
  0.0 84.2 jit_solution(13287708469286292087)
XLA Ops:
  0.0 82.4 %shard_map.127 = bf16[96,2048]{1,0:T(8,128)(2,1)} custom-call(bf16[384,512]{1,0:T(8,128)(2,1)} %tok.1, f32[1,2048]{1,0:T(1,128)} %bitcast.1, bf16[256,512]{1,0:T(8,128)(2,1)} %wpi.1, bf16[256,512]{1,0:T(8,128)(2,1)} %wli.1, bf16[1,512,512]{2,1,0:T(8,128)(2,1)} %mix_in.1, bf16[4,512]{1,0:T(4,128)(2,1)} %taps_in.1, bf16[2,4,128,128]{3,2,1,0:T(8,128)(2,1)} %rec_in.1, ...), custom_call_target="tpu_custom_call" | custom-call | tf_op jit(solution)/shard_map/pallas_call | solution.py:1166
  82.4 1.8 %copy.15 = bf16[96,2048]{1,0:T(8,128)(2,1)} copy(bf16[96,2048]{1,0:T(8,128)(2,1)} %shard_map.127) | data formatting | bytes 786432

commit v5 on v4

--- a/solution.py
+++ b/solution.py
@@ -886,7 +886,7 @@
         gate_stage(wide, taps, rec, ing, rate, decay, keep, drive, count, some)
 
     gates(range(heads // 2))
-    small = group < tp // 2
+    small = group < tp - 1
 
     @pl.when(keep_order)
     def _():

time: 85.4 us -> 85.4 us (level)
  no operation moved by 1% of the time
where the time goes in v5:
time: 85.4 us; the launch traced here: 84.2 us
  Pallas kernels  82.4 us (96%)
  local copies, waits for them, and re-layouts  1.77 us (2%)
    pallas_call x1, Pallas kernels, per_device(): pl.pallas_call(functools.partial(layer_kernel, sp=sp, tp=tp), out_shape=j...  82.4 us
    unnamed x1, local copies, waits for them, and re-layouts  1.77 us

profile of v5, /device:TPU:3, one launch (start us, length us, event | category | flops | bytes accessed | tf_op | source)
XLA Modules:
  0.0 84.2 jit_solution(1505273289418056031)
XLA Ops:
  0.0 82.4 %shard_map.127 = bf16[96,2048]{1,0:T(8,128)(2,1)} custom-call(bf16[384,512]{1,0:T(8,128)(2,1)} %tok.1, f32[1,2048]{1,0:T(1,128)} %bitcast.1, bf16[256,512]{1,0:T(8,128)(2,1)} %wpi.1, bf16[256,512]{1,0:T(8,128)(2,1)} %wli.1, bf16[1,512,512]{2,1,0:T(8,128)(2,1)} %mix_in.1, bf16[4,512]{1,0:T(4,128)(2,1)} %taps_in.1, bf16[2,4,128,128]{3,2,1,0:T(8,128)(2,1)} %rec_in.1, ...), custom_call_target="tpu_custom_call" | custom-call | tf_op jit(solution)/shard_map/pallas_call | solution.py:1166
  82.4 1.8 %copy.15 = bf16[96,2048]{1,0:T(8,128)(2,1)} copy(bf16[96,2048]{1,0:T(8,128)(2,1)} %shard_map.127) | data formatting | bytes 786432
